TPU v7x, 512 devices: a whole 4x8x8 slice. The times are simulated.
512 devices in a mesh: sp: 32 (over z, x), tp: 16 (over y, core).
Axes of the slice: x: 4, y: 8, z: 8, core: 2. Of those that a mesh axis runs over, the one named last changes fastest.
Arguments:
- queries: bfloat16 [4096, 2048], P('sp', 'tp'), may hold values from -15 to 15
- key_rows: bfloat16 [4096, 2048], P('sp', 'tp'), may hold values from -6 to 6
- value_rows: bfloat16 [4096, 2048], P('sp', 'tp'), may hold values from -6 to 6
- break_bias: bfloat16 [4096, 16], P('sp', 'tp'), may hold values from -14 to 1
- stream: bfloat16 [4096, 4096], P('sp', 'tp'), may hold values from -24 to 24
- out_proj: bfloat16 [2048, 4096], P(None, 'tp'), may hold values from -0.5 to 0.5
- norm_gain: float32 [4096], P('tp'), may hold values from 0.1 to 1.9
- expert_ids: int32 [4096, 2], P('sp'), may hold values from 0 to 63, all different within a row; in each aligned block of 128 rows (0 to 127, 128 to 255, ...) at most 8 rows name the same one
- route_weights: float32 [4096, 2], P('sp'), may hold values from 0.1 to 2.5
- gate_proj: bfloat16 [64, 4096, 384], P('sp', 'tp'), may hold values from -0.09375 to 0.09375
- up_proj: bfloat16 [64, 4096, 384], P('sp', 'tp'), may hold values from -0.09375 to 0.09375
- down_proj: bfloat16 [64, 384, 4096], P('sp', None, 'tp'), may hold values from -0.3125 to 0.3125
- shared_gate: bfloat16 [4096, 384], P('tp'), may hold values from -0.09375 to 0.09375
- shared_up: bfloat16 [4096, 384], P('tp'), may hold values from -0.09375 to 0.09375
- shared_down: bfloat16 [384, 4096], P(None, 'tp'), may hold values from -0.3125 to 0.3125
Outputs:
- result: bfloat16 [4096, 4096], P('sp', 'tp')
Inputs may be any that keep to these rules, and one draw needn't show every extreme that they name: `expert_ids`: each row names 2 different experts; within the rows of one index of sp no expert is named by more than 8 rows, a bound that some block reaches of them.
All inputs are finite; a program needn't handle non-finite values.
Results may differ from a plain program's by a relative error of at most 0.022.
Values may be sent and summed in bfloat16 or wider, within the bound.
A program may use at most 64 MiB of HBM per device.

v0:
```python
import jax
import jax.numpy as jnp
from jax import lax
from jax.sharding import PartitionSpec as P

D = 4096


EPS = 1e-06
row_block_size = 32


def sent_together(arrays, axis, dim, along):
    widths = [a.shape[along] for a in arrays]
    both = jnp.concatenate(arrays, axis=along)
    filled = lax.all_gather(both, axis, axis=dim, tiled=True)
    return tuple(jnp.split(filled, [sum(widths[:k]) for k in range(1, len(widths))], axis=along))


def from_everyone(value, axis):
    copies = jnp.broadcast_to(value, (lax.axis_size(axis), *value.shape))
    return lax.all_to_all(copies, axis, split_axis=0, concat_axis=0, tiled=True)


def joined_along(blocks, dim):
    shape = list(blocks.shape[1:])
    shape[dim] *= blocks.shape[0]
    return jnp.moveaxis(blocks, 0, dim).reshape(shape)


def collect(value, axis, dim):
    blocks = from_everyone(value, axis)
    return joined_along(blocks, dim)


def taken_together(value, axis):
    return from_everyone(value, axis).sum(axis=0)


def cut_along(value, dim, peers):
    shape = value.shape
    blocks = value.reshape(*shape[:dim], peers, shape[dim] // peers, *shape[dim + 1 :])
    return jnp.moveaxis(blocks, dim, 0)


def summed_on_arrival(value, axis, dim):
    blocks = cut_along(value, dim, lax.axis_size(axis))
    arrived = lax.all_to_all(blocks, axis, split_axis=0, concat_axis=0, tiled=True)
    return arrived.astype(jnp.float32).sum(axis=0)


def side_by_side(arrays, axis, dim, along):
    ends, at = ([], 0)
    for a in arrays[:-1]:
        at += a.shape[along]
        ends.append(at)
    both = jnp.concatenate(arrays, axis=along)
    return tuple(jnp.split(summed_on_arrival(both, axis, dim), ends, axis=along))


def gather_packed(arrays, axis, dims):
    line = jnp.concatenate([a.reshape(-1) for a in arrays])
    lines, at, outs = (lax.all_gather(line, axis), 0, [])
    for a, dim in zip(arrays, dims):
        blocks = lines[:, at : at + a.size].reshape(-1, *a.shape)
        outs.append(joined_along(blocks, dim))
        at += a.size
    return tuple(outs)


def block_terms(query_heads, key_piece, value_piece, bias_piece, query_pos):
    heads_local = query_heads.shape[1]
    head_dim = query_heads.shape[2]
    key_count = key_piece.shape[0]
    key_heads = key_piece.reshape(key_count, heads_local, head_dim)
    value_heads = value_piece.reshape(key_count, heads_local, head_dim).astype(jnp.float32)
    logits = jnp.einsum("thd,shd->hts", query_heads, key_heads, preferred_element_type=jnp.float32)
    logits = logits * head_dim ** (-0.5) + bias_piece.astype(jnp.float32).T[:, None, :]
    key_pos = jnp.arange(key_count, dtype=jnp.int32)
    before = (key_pos[None, :] < query_pos[:, None])[None]
    log_fail = jnp.where(before, jax.nn.log_sigmoid(-logits), 0.0)
    tail_sum = lax.cumsum(log_fail, axis=2, reverse=True) - log_fail
    weights = jnp.where(before, jnp.exp(jax.nn.log_sigmoid(logits) + tail_sum), 0.0)
    summary = jnp.einsum("hts,shd->thd", weights, value_heads)
    return (summary, jnp.sum(log_fail, axis=2).T)


def body(
    queries,
    key_rows,
    value_rows,
    break_bias,
    stream,
    out_proj,
    norm_gain,
    expert_ids,
    route_weights,
    gate_proj,
    up_proj,
    down_proj,
    shared_gate,
    shared_up,
    shared_down,
):
    tok_dev = queries.shape[0]
    heads_local = break_bias.shape[1]
    head_dim = queries.shape[1] // heads_local
    blocks_all = lax.axis_size("sp")
    own_block = lax.axis_index("sp")
    own_start = own_block * tok_dev
    query_pos = own_start + jnp.arange(tok_dev, dtype=jnp.int32)
    query_heads = queries.reshape(tok_dev, heads_local, head_dim)
    row_step = min(row_block_size, tok_dev)
    row_turns = tok_dev // row_step
    empty_sums = jnp.zeros((blocks_all, tok_dev, heads_local, head_dim), jnp.float32)
    empty_fails = jnp.zeros((blocks_all, tok_dev, heads_local), jnp.float32)
    offset = jnp.int32(0)
    key_piece, value_piece, bias_piece = sent_together(
        (key_rows, value_rows, break_bias), "sp", 0, 1
    )
    block_id = offset // tok_dev

    def compute(operand):

        def rows_part(turn):
            row_start = turn * row_step
            part_q = lax.dynamic_slice_in_dim(query_heads, row_start, row_step, 0)
            part_pos = lax.dynamic_slice_in_dim(query_pos, row_start, row_step, 0)
            return block_terms(part_q, key_piece, value_piece, bias_piece, part_pos)

        summary, fail_sum = lax.map(rows_part, jnp.arange(row_turns, dtype=jnp.int32))
        return (
            summary.reshape(tok_dev, heads_local, head_dim),
            fail_sum.reshape(tok_dev, heads_local),
        )

    def skip(operand):
        return (
            jnp.zeros((tok_dev, heads_local, head_dim), jnp.float32),
            jnp.zeros((tok_dev, heads_local), jnp.float32),
        )

    summary, fail_sum = lax.cond(offset < own_start + tok_dev, compute, skip, 0)
    sums_in = empty_sums
    fails_in = empty_fails
    sums_in = lax.dynamic_update_index_in_dim(sums_in, summary, block_id, 0)
    fails_in = lax.dynamic_update_index_in_dim(fails_in, fail_sum, block_id, 0)
    later_fail = jnp.cumsum(fails_in[::-1], axis=0)[::-1] - fails_in
    attended = jnp.sum(jnp.exp(later_fail)[..., None] * sums_in, axis=0)
    attended = attended.reshape(tok_dev, heads_local * head_dim).astype(jnp.bfloat16)
    projected = jnp.dot(collect(attended, "tp", 1), out_proj, preferred_element_type=jnp.float32)
    mixed = (stream.astype(jnp.float32) + projected).astype(jnp.bfloat16)
    mixed = lax.optimization_barrier(mixed)
    mixed_f = mixed.astype(jnp.float32)
    square_sum = taken_together(jnp.sum(mixed_f * mixed_f, axis=1), "tp")
    inv_rms = lax.rsqrt(square_sum / D + EPS)
    normed = (mixed_f * inv_rms[:, None] * norm_gain[None, :]).astype(jnp.bfloat16)
    experts_local = gate_proj.shape[0]
    experts_all = experts_local * blocks_all
    top_k = expert_ids.shape[1]
    capacity = 2 * top_k * tok_dev // experts_all
    flat_ids = expert_ids.reshape(-1)
    one_hot = (flat_ids[:, None] == jnp.arange(experts_all, dtype=jnp.int32)[None, :]).astype(
        jnp.int32
    )
    ranks = jnp.sum((jnp.cumsum(one_hot, axis=0) - one_hot) * one_hot, axis=1)
    owner = flat_ids // experts_local
    local_id = flat_ids % experts_local
    slot_index = local_id * (blocks_all * capacity) + owner * capacity + ranks
    token_index = jnp.arange(tok_dev * top_k, dtype=jnp.int32) // top_k
    token_of_slot = (
        jnp.full((experts_all * capacity,), tok_dev, jnp.int32).at[slot_index].set(token_index)
    )
    padded_rows = jnp.concatenate([normed, jnp.zeros((1, normed.shape[1]), jnp.bfloat16)], 0)
    send_rows = padded_rows[token_of_slot].reshape(
        experts_local, blocks_all * capacity, normed.shape[1]
    )
    arrived = lax.all_to_all(send_rows, "sp", split_axis=1, concat_axis=1, tiled=True)
    gate_part = jnp.einsum("erd,edf->erf", arrived, gate_proj, preferred_element_type=jnp.float32)
    up_part = jnp.einsum("erd,edf->erf", arrived, up_proj, preferred_element_type=jnp.float32)
    routed_rows = experts_local * blocks_all * capacity
    gate_part = gate_part.reshape(routed_rows, -1)
    up_part = up_part.reshape(routed_rows, -1)
    shared_gate_part = jnp.dot(normed, shared_gate, preferred_element_type=jnp.float32)
    shared_up_part = jnp.dot(normed, shared_up, preferred_element_type=jnp.float32)
    gate_share, up_share, sgate_share, sup_share = (
        *side_by_side((gate_part.astype(jnp.bfloat16), up_part.astype(jnp.bfloat16)), "tp", 0, 1),
        *side_by_side(
            (shared_gate_part.astype(jnp.bfloat16), shared_up_part.astype(jnp.bfloat16)), "tp", 0, 1
        ),
    )
    hidden_share = (jax.nn.silu(gate_share) * up_share).astype(jnp.bfloat16)
    shared_share = (jax.nn.silu(sgate_share) * sup_share).astype(jnp.bfloat16)
    hidden, shared_hidden = gather_packed((hidden_share, shared_share), "tp", (0, 0))
    hidden = hidden.reshape(experts_local, blocks_all * capacity, -1)
    expert_out = jnp.einsum(
        "erf,efd->erd", hidden, down_proj, preferred_element_type=jnp.float32
    ).astype(jnp.bfloat16)
    returned = lax.all_to_all(expert_out, "sp", split_axis=1, concat_axis=1, tiled=True)
    flat_back = returned.reshape(experts_all * capacity, -1)
    picked = flat_back[slot_index.reshape(tok_dev, top_k)]
    routed = jnp.einsum("tk,tkd->td", route_weights, picked.astype(jnp.float32))
    shared_out = jnp.dot(shared_hidden, shared_down, preferred_element_type=jnp.float32)
    return (mixed_f + shared_out + routed).astype(jnp.bfloat16)


def solution(mesh):
    in_specs = (
        P("sp", "tp"),
        P("sp", "tp"),
        P("sp", "tp"),
        P("sp", "tp"),
        P("sp", "tp"),
        P(None, "tp"),
        P("tp"),
        P("sp", None),
        P("sp", None),
        P("sp", "tp", None),
        P("sp", "tp", None),
        P("sp", None, "tp"),
        P("tp", None),
        P("tp", None),
        P(None, "tp"),
    )
    out_specs = P("sp", "tp")
    return jax.shard_map(body, mesh=mesh, in_specs=in_specs, out_specs=out_specs, check_vma=False)
```

profile of v0, /device:TPU:1, one launch (start us, length us, event | category | flops | bytes accessed | tf_op | source)
XLA Modules:
  0.0 440.3 jit_solution(7422359589462972336)
XLA Ops:
  6.5 0.9 copy.71
  7.4 1.4 pad_maximum_fusion.1
  8.9 0.8 copy.74
  10.1 87.4 %all-gather.3.cloned.1.call-done = bf16[4096,257]{1,0:T(8,128)(2,1)} async-done(((bf16[128,257]{1,0:T(8,128)(2,1)}), bf16[4096,257]{1,0:T(8,128)(2,1)}) %all-gather.3.cloned.1.call-update) | async-done | bytes 2105360 | tf_op jit(solution)/shard_map/all_gather | solution.py:16
  97.4 195.9 %conditional.1 = (f32[32,128,1,128]{3,1,2,0:T(8,128)}, f32[32,128,1]{1,2,0:T(1,128)S(1)}) conditional(s32[]{:T(128)} %convert_element_type.78, () %tuple.25, (bf16[128,128]{1,0:T(8,128)(2,1)}, s32[]{:T(128)}, s32[128]{0:T(128)S(1)}, bf16[4096,257]{1,0:T(8,128)(2,1)}) %tuple.26), branch_computations={%region_0.1_spmd, %region_1.7_spmd} | conditional | flops 88117312 | bytes 18565128 | solution.py:143
  97.4 3.0 fusion.57
  100.5 3.0 copy.70
  103.6 186.8 %while.11 = (s32[]{:T(128)}, f32[4,32,1,128]{3,1,2,0:T(8,128)S(1)}, f32[4,32,1]{1,2,0:T(1,128)S(1)}, s32[4]{0:T(128)S(1)}, s32[128]{0:T(128)S(1)}, /*index=5*/bf...) while((s32[]{:T(128)}, f32[4,32,1,128]{3,1,2,0:T(8,128)S(1)}, ...), condition=%wide.region_6.6_spmd, body=%wide.region_2.5_spmd.sunk | while | flops 88117184 | bytes 7960919 | solution.py:131
  103.6 0.7 dynamic_slice.18
  104.9 1.7 fusion.88
  106.7 0.5 fusion.89
  107.3 39.8 %reduce-window.24 = f32[1,32,32,128]{3,2,1,0:T(8,128)S(1)} reduce-window(f32[1,32,32,128]{3,2,1,0:T(8,128)S(1)} %bitcast.123, f32[]{:T(128)} %constant.126.clone..sunk), window={size=1x1x1x128 pad=0_0x0_0x0_0x0_127}, to_apply=%region_3.2 | reduce-window | flops 16646144 | bytes 1048580 | tf_op jit(solution)/shard_map/reduce-window
  147.4 0.2 reduce-window.25
  147.9 2.4 fusion.90
  150.3 0.7 dynamic_slice.18
  151.6 1.7 fusion.88
  153.4 0.5 fusion.89
  154.0 39.8 %reduce-window.24 = f32[1,32,32,128]{3,2,1,0:T(8,128)S(1)} reduce-window(f32[1,32,32,128]{3,2,1,0:T(8,128)S(1)} %bitcast.123, f32[]{:T(128)} %constant.126.clone..sunk), window={size=1x1x1x128 pad=0_0x0_0x0_0x0_127}, to_apply=%region_3.2 | reduce-window | flops 16646144 | bytes 1048580 | tf_op jit(solution)/shard_map/reduce-window
  194.1 0.2 reduce-window.25
  194.6 2.4 fusion.90
  197.0 0.7 dynamic_slice.18
  198.4 1.7 fusion.88
  200.1 0.5 fusion.89
  200.7 39.8 %reduce-window.24 = f32[1,32,32,128]{3,2,1,0:T(8,128)S(1)} reduce-window(f32[1,32,32,128]{3,2,1,0:T(8,128)S(1)} %bitcast.123, f32[]{:T(128)} %constant.126.clone..sunk), window={size=1x1x1x128 pad=0_0x0_0x0_0x0_127}, to_apply=%region_3.2 | reduce-window | flops 16646144 | bytes 1048580 | tf_op jit(solution)/shard_map/reduce-window
  240.8 0.2 reduce-window.25
  241.3 2.4 fusion.90
  243.7 0.7 dynamic_slice.18
  245.1 1.7 fusion.88
  246.9 0.5 fusion.89
  247.4 39.8 %reduce-window.24 = f32[1,32,32,128]{3,2,1,0:T(8,128)S(1)} reduce-window(f32[1,32,32,128]{3,2,1,0:T(8,128)S(1)} %bitcast.123, f32[]{:T(128)} %constant.126.clone..sunk), window={size=1x1x1x128 pad=0_0x0_0x0_0x0_127}, to_apply=%region_3.2 | reduce-window | flops 16646144 | bytes 1048580 | tf_op jit(solution)/shard_map/reduce-window
  288.0 2.4 fusion.90
  290.4 1.6 dynamic_update_slice.18
  292.1 0.6 broadcast.224
  292.6 0.7 reduce.11
  293.5 2.0 multiply_reduce_fusion
  295.6 0.9 broadcast_in_dim.49
  296.5 11.4 %all-to-all-start = ((bf16[16,128,128]{1,2,0:T(8,128)(2,1)}), bf16[16,128,128]{1,2,0:T(8,128)(2,1)S(1)}, u32[]{:S(2)}, u32[]{:S(2)}) async-start(bf16[16,128,128]{1,2,0:T(8,128)(2,1)} %broadcast_in_dim.49), calls=%async_computation | async-start | bytes 1048576 | tf_op jit(solution)/shard_map/all_to_all | solution.py:22
  307.9 0.6 reduce-window.16
  308.9 1.4 scatter_custom_fusion
  310.3 14.8 %all-to-all-done = bf16[16,128,128]{1,2,0:T(8,128)(2,1)S(1)} async-done(((bf16[16,128,128]{1,2,0:T(8,128)(2,1)}), bf16[16,128,128]{1,2,0:T(8,128)(2,1)S(1)}, u32[]{:S(2)}, u32[]{:S(2)}) %all-to-all-start) | async-done | bytes 524320 | tf_op jit(solution)/shard_map/all_to_all | solution.py:22
  325.1 0.4 fusion.31
  325.6 0.6 broadcast_in_dim.50
  326.3 3.4 all-to-all-start.1
  329.7 6.6 %all-to-all-done.1 = f32[16,1,128]{2,1,0:T(1,128)S(1)} async-done(((f32[16,1,128]{2,1,0:T(1,128)}), f32[16,1,128]{2,1,0:T(1,128)S(1)}, u32[]{:S(2)}, u32[]{:S(2)}) %all-to-all-start.1) | async-done | bytes 8224 | tf_op jit(solution)/shard_map/all_to_all | solution.py:22
  336.4 2.0 gather_fusion
  338.3 1.0 copy.78
  339.3 5.1 %all-to-all-start.2 = ((bf16[2,256,256]{2,0,1:T(2,128)(2,1)}), bf16[2,256,256]{2,0,1:T(2,128)(2,1)S(1)}, u32[]{:S(2)}, u32[]{:S(2)}) async-start(bf16[2,256,256]{2,0,1:T(2,128)(2,1)} %copy.78), calls=%async_computation.2 | async-start | bytes 524288 | tf_op jit(solution)/shard_map/all_to_all | solution.py:178
  344.8 0.7 maximum_bitcast_fusion
  345.5 10.2 %all-to-all-done.2 = bf16[2,256,256]{2,0,1:T(2,128)(2,1)S(1)} async-done(((bf16[2,256,256]{2,0,1:T(2,128)(2,1)}), bf16[2,256,256]{2,0,1:T(2,128)(2,1)S(1)}, u32[]{:S(2)}, u32[]{:S(2)}) %all-to-all-start.2) | async-done | bytes 262176 | tf_op jit(solution)/shard_map/all_to_all | solution.py:178
  355.7 5.8 %all-to-all-start.4 = ((bf16[16,8,768]{2,1,0:T(8,128)(2,1)}), bf16[16,8,768]{2,1,0:T(8,128)(2,1)S(1)}, u32[]{:S(2)}, u32[]{:S(2)}) async-start(bf16[16,8,768]{2,1,0:T(8,128)(2,1)} %maximum_bitcast_fusion), calls=%async_computation.4 | async-start | bytes 393216 | tf_op jit(solution)/shard_map/all_to_all | solution.py:48
  361.5 0.3 convolution_convert_fusion.1
  361.8 0.3 convolution_convert_fusion
  362.1 1.0 pad_maximum_fusion
  363.1 8.7 %all-to-all-done.4 = bf16[16,8,768]{2,1,0:T(8,128)(2,1)S(1)} async-done(((bf16[16,8,768]{2,1,0:T(8,128)(2,1)}), bf16[16,8,768]{2,1,0:T(8,128)(2,1)S(1)}, u32[]{:S(2)}, u32[]{:S(2)}) %all-to-all-start.4) | async-done | bytes 196640 | tf_op jit(solution)/shard_map/all_to_all | solution.py:48
  371.8 3.5 all-to-all-start.3
  375.5 21.8 %all-to-all-done.3 = bf16[16,32,768]{2,1,0:T(8,128)(2,1)S(1)} async-done(((bf16[16,32,768]{2,1,0:T(8,128)(2,1)}), bf16[16,32,768]{2,1,0:T(8,128)(2,1)S(1)}, u32[]{:S(2)}, u32[]{:S(2)}) %all-to-all-start.3) | async-done | bytes 786464 | tf_op jit(solution)/shard_map/all_to_all | solution.py:48
  397.5 15.8 %all-gather = bf16[245760]{0:T(1024)(128)(2,1)S(1)} all-gather(bf16[15360]{0:T(1024)(128)(2,1)S(1)} %pad_maximum_fusion.2), channel_id=2, replica_groups=mesh['sp'=32,'tp'=16] {'tp'}, dimensions={0}, use_global_device_ids=true | all-gather | bytes 522240 | tf_op jit(solution)/shard_map/all_gather | solution.py:63
  413.8 0.3 convolution_convert_fusion.2
  414.1 1.0 copy.81
  415.1 4.0 all-to-all-start.5
  419.7 11.3 %all-to-all-done.5 = bf16[2,256,256]{2,0,1:T(2,128)(2,1)S(1)} async-done(((bf16[2,256,256]{2,0,1:T(2,128)(2,1)}), bf16[2,256,256]{2,0,1:T(2,128)(2,1)S(1)}, u32[]{:S(2)}, u32[]{:S(2)}) %all-to-all-start.5) | async-done | bytes 262176 | tf_op jit(solution)/shard_map/all_to_all | solution.py:199
  431.1 1.2 gather_fusion.1
  432.3 0.3 fusion.59
  432.6 0.8 fusion.32
  (105 shorter events, 6.2 us)
Async XLA Ops:
  6.5 318.6 %copy-start = (bf16[2048,256]{1,0:T(8,128)(2,1)S(1)}, bf16[2048,256]{1,0:T(8,128)(2,1)}, u32[]{:S(2)}) copy-start(bf16[2048,256]{1,0:T(8,128)(2,1)} %param.24) | copy-start | bytes 3145732
  6.5 90.9 %all-gather.3.cloned.1.call-start = ((), (), s32[]{:S(2)}) async-start(), calls=%async_computation.6 | async-start | bytes 3244032 | tf_op jit(solution)/shard_map/all_gather | solution.py:16
  293.5 31.6 %copy-start.7 = (bf16[128,256]{1,0:T(8,128)(2,1)S(1)}, bf16[128,256]{1,0:T(8,128)(2,1)}, u32[]{:S(2)}) copy-start(bf16[128,256]{1,0:T(8,128)(2,1)} %param.23) | copy-start | bytes 196612
  295.5 40.8 %copy-start.8 = (f32[256]{0:T(256)S(1)}, f32[256]{0:T(256)}, u32[]{:S(2)}) copy-start(f32[256]{0:T(256)} %param.25) | copy-start | bytes 3076
  296.5 28.6 %all-to-all-start = ((bf16[16,128,128]{1,2,0:T(8,128)(2,1)}), bf16[16,128,128]{1,2,0:T(8,128)(2,1)S(1)}, u32[]{:S(2)}, u32[]{:S(2)}) async-start(bf16[16,128,128]{1,2,0:T(8,128)(2,1)} %broadcast_in_dim.49), calls=%async_computation | async-start | bytes 1048576 | tf_op jit(solution)/shard_map/all_to_all | solution.py:22
  325.5 18.9 %copy-start.5 = (bf16[256,384]{1,0:T(8,128)(2,1)S(1)}, bf16[256,384]{1,0:T(8,128)(2,1)}, u32[]{:S(2)}) copy-start(bf16[256,384]{1,0:T(8,128)(2,1)} %param.32) | copy-start | bytes 589828
  325.5 19.1 %copy-start.6 = (bf16[256,384]{1,0:T(8,128)(2,1)S(1)}, bf16[256,384]{1,0:T(8,128)(2,1)}, u32[]{:S(2)}) copy-start(bf16[256,384]{1,0:T(8,128)(2,1)} %param.31) | copy-start | bytes 589828
  326.3 10.0 %all-to-all-start.1 = ((f32[16,1,128]{2,1,0:T(1,128)}), f32[16,1,128]{2,1,0:T(1,128)S(1)}, u32[]{:S(2)}, u32[]{:S(2)}) async-start(f32[16,1,128]{2,1,0:T(1,128)} %broadcast_in_dim.50), calls=%async_computation.1 | async-start | bytes 16384 | tf_op jit(solution)/shard_map/all_to_all | solution.py:22
  336.4 25.2 %copy-start.1 = (bf16[2,256,384]{2,1,0:T(8,128)(2,1)S(1)}, bf16[2,256,384]{2,1,0:T(8,128)(2,1)}, u32[]{:S(2)}) copy-start(bf16[2,256,384]{2,1,0:T(8,128)(2,1)} %param.28) | copy-start | bytes 1179652
  338.3 23.5 %copy-start.2 = (bf16[2,256,384]{2,1,0:T(8,128)(2,1)S(1)}, bf16[2,256,384]{2,1,0:T(8,128)(2,1)}, u32[]{:S(2)}) copy-start(bf16[2,256,384]{2,1,0:T(8,128)(2,1)} %param.29) | copy-start | bytes 1179652
  339.3 16.4 %all-to-all-start.2 = ((bf16[2,256,256]{2,0,1:T(2,128)(2,1)}), bf16[2,256,256]{2,0,1:T(2,128)(2,1)S(1)}, u32[]{:S(2)}, u32[]{:S(2)}) async-start(bf16[2,256,256]{2,0,1:T(2,128)(2,1)} %copy.78), calls=%async_computation.2 | async-start | bytes 524288 | tf_op jit(solution)/shard_map/all_to_all | solution.py:178
  355.7 16.0 %all-to-all-start.4 = ((bf16[16,8,768]{2,1,0:T(8,128)(2,1)}), bf16[16,8,768]{2,1,0:T(8,128)(2,1)S(1)}, u32[]{:S(2)}, u32[]{:S(2)}) async-start(bf16[16,8,768]{2,1,0:T(8,128)(2,1)} %maximum_bitcast_fusion), calls=%async_computation.4 | async-start | bytes 393216 | tf_op jit(solution)/shard_map/all_to_all | solution.py:48
  371.8 25.6 %all-to-all-start.3 = ((bf16[16,32,768]{2,1,0:T(8,128)(2,1)}), bf16[16,32,768]{2,1,0:T(8,128)(2,1)S(1)}, u32[]{:S(2)}, u32[]{:S(2)}) async-start(bf16[16,32,768]{2,1,0:T(8,128)(2,1)} %pad_maximum_fusion), calls=%async_computation.3 | async-start | bytes 1572864 | tf_op jit(solution)/shard_map/all_to_all | solution.py:48
  375.5 38.3 %copy-start.3 = (bf16[2,384,256]{2,1,0:T(8,128)(2,1)S(1)}, bf16[2,384,256]{2,1,0:T(8,128)(2,1)}, u32[]{:S(2)}) copy-start(bf16[2,384,256]{2,1,0:T(8,128)(2,1)} %param.30) | copy-start | bytes 1179652
  413.4 5.8 %copy-start.9 = (s32[128,2]{0,1:T(2,128)S(1)}, s32[128,2]{0,1:T(2,128)}, u32[]{:S(2)}) copy-start(s32[128,2]{0,1:T(2,128)} %param.26) | copy-start | bytes 3076
  413.6 5.9 %copy-start.10 = (f32[128,2]{0,1:T(2,128)S(1)}, f32[128,2]{0,1:T(2,128)}, u32[]{:S(2)}) copy-start(f32[128,2]{0,1:T(2,128)} %param.27) | copy-start | bytes 3076
  415.1 17.5 %copy-start.4 = (bf16[384,256]{1,0:T(8,128)(2,1)S(1)}, bf16[384,256]{1,0:T(8,128)(2,1)}, u32[]{:S(2)}) copy-start(bf16[384,256]{1,0:T(8,128)(2,1)} %param.33) | copy-start | bytes 589828
  415.1 16.0 %all-to-all-start.5 = ((bf16[2,256,256]{2,0,1:T(2,128)(2,1)}), bf16[2,256,256]{2,0,1:T(2,128)(2,1)S(1)}, u32[]{:S(2)}, u32[]{:S(2)}) async-start(bf16[2,256,256]{2,0,1:T(2,128)(2,1)} %copy.81), calls=%async_computation.5 | async-start | bytes 524288 | tf_op jit(solution)/shard_map/all_to_all | solution.py:199
Sparse Core Ops, SparseCore 0:
  10.5 86.8 all-gather.2
where the time goes:
time: 441 us; the launch traced here: 440 us
  other arithmetic  169 us (38%)
  waiting for transfers between devices  161 us (37%)
  starting transfers between devices  33.2 us (8%)
  local copies, waits for them, and re-layouts  25.3 us (6%)
  matrix products  19.2 us (4%)
  blocking collectives  15.8 us (4%)
  between operations  13.8 us (3%)
    another operation x12, other arithmetic  161 us
    all_gather x1, waiting for transfers between devices, sent_together(): filled = lax.all_gather(both, axis, axis=dim, tiled=True)  87.4 us
    all_to_all x2, waiting for transfers between devices, summed_on_arrival(): lax.all_to_all(blocks, axis, split_axis=0, concat_axis=0, tiled=True)  30.5 us
    all_to_all x2, waiting for transfers between devices, from_everyone(): return lax.all_to_all(copies, axis, split_axis=0, concat_axis=0, tiled=True)  21.4 us
    all_gather x1, blocking collectives, gather_packed(): lines, at, outs = (lax.all_gather(line, axis), 0, [])  15.8 us
    all_to_all x2, starting transfers between devices, from_everyone(): return lax.all_to_all(copies, axis, split_axis=0, concat_axis=0, tiled=True)  14.8 us
    all_to_all x1, waiting for transfers between devices, body(): lax.all_to_all(expert_out, 'sp', split_axis=1, concat_axis=1, tiled=True)  11.3 us
    all_to_all x1, waiting for transfers between devices, body(): lax.all_to_all(send_rows, 'sp', split_axis=1, concat_axis=1, tiled=True)  10.2 us
  transfers between devices with their start and end apart: 7, of which 7 were waited for; matrix products, arithmetic and copies ran while one was open for 2% of the time, Pallas kernels for 0%

commit v1 on v0

v1 whole, which is shorter than its diff:
```python
import functools

import jax
import jax.numpy as jnp
from jax import lax
from jax.experimental import pallas as pl
from jax.experimental.pallas import tpu as pltpu
from jax.sharding import PartitionSpec as P

EPS = 1e-06
NX = 4
MESH = pl.DeviceIdType.MESH
F32, BF16 = jnp.float32, jnp.bfloat16


def rdma(src, dst, send, recv, device):
    return pltpu.make_async_remote_copy(
        src_ref=src, dst_ref=dst, send_sem=send, recv_sem=recv, device_id=device, device_id_type=MESH
    )


def each(low, high, fn):
    def turn(i, carry):
        fn(i)
        return carry

    lax.fori_loop(low, high, turn, 0)


def offset_near(i, n):
    half = i // 2 + 1
    return jnp.where(lax.rem(i, 2) == 0, half, n - half)


def dot(a, b):
    return jnp.dot(a, b, preferred_element_type=F32)


def dot_nt(a, b):
    return lax.dot_general(a, b, (((1,), (1,)), ((), ())), preferred_element_type=F32)


def halves(value):
    high = value.astype(BF16)
    return high, (value - high.astype(F32)).astype(BF16)


def iota(shape, dim):
    return lax.broadcasted_iota(jnp.int32, shape, dim)


def layer_kernel(
    sizes,
    q_ref,
    k_ref,
    v_ref,
    b_ref,
    stream_ref,
    gain_ref,
    ids_ref,
    rw_ref,
    wo_hbm,
    wg_hbm,
    wu_hbm,
    wd_hbm,
    sg_hbm,
    su_hbm,
    sd_hbm,
    out_ref,
    wo,
    wg,
    wu,
    wd,
    sg,
    su,
    sd,
    kv,
    qbuf,
    part_out,
    part_in,
    tri,
    abuf,
    pt,
    w_hi,
    w_lo,
    mixed_ref,
    snd,
    arr,
    part,
    pre,
    red,
    rs_in,
    spart,
    spre,
    sred,
    srs_in,
    hbuf,
    shbuf,
    ret_out,
    ret_in,
    load_sem,
    kv_send,
    kv_recv,
    q_send,
    q_recv,
    p_send,
    p_recv,
    a_send,
    a_recv,
    af_send,
    af_recv,
    d_send,
    d_recv,
    pre_send,
    pre_recv,
    rs_send,
    rs_recv,
    spre_send,
    spre_recv,
    srs_send,
    srs_recv,
    h_send,
    h_recv,
    hf_send,
    hf_recv,
    sh_send,
    sh_recv,
    shf_send,
    shf_recv,
    r_send,
    r_recv,
):
    nz, nx, ny = sizes
    nsp, ntp = nz * nx, ny * 2
    tok, hd = q_ref.shape
    feat = stream_ref.shape[1]
    ffe = wg.shape[1]
    nslot = nsp * snd.shape[1]
    per_dest = snd.shape[1]
    cap = per_dest // 2
    nexp = nsp * 2
    width = feat * ntp
    sp, tp = lax.axis_index("sp"), lax.axis_index("tp")
    z, x = sp // nx, lax.rem(sp, nx)
    y, c = tp // 2, lax.rem(tp, 2)
    partner = (sp, y * 2 + 1 - c)

    def in_column(yy):
        return (sp, yy * 2 + c)

    loads = [
        pltpu.make_async_copy(src, dst, load_sem.at[i])
        for i, (src, dst) in enumerate(
            [(wo_hbm, wo), (sg_hbm, sg), (su_hbm, su), (wg_hbm, wg), (wu_hbm, wu), (sd_hbm, sd), (wd_hbm, wd)]
        )
    ]

    barrier = pltpu.get_barrier_semaphore()

    def greet_sp(i):
        pl.semaphore_signal(
            barrier, inc=1, device_id=(lax.rem(sp + i, nsp), tp), device_id_type=MESH
        )

    def greet_tp(i):
        pl.semaphore_signal(barrier, inc=1, device_id=in_column(lax.rem(y + i, ny)), device_id_type=MESH)

    each(1, nsp, greet_sp)
    each(1, ny, greet_tp)
    pl.semaphore_signal(barrier, inc=1, device_id=partner, device_id_type=MESH)
    for copy in loads:
        copy.start()

    eye = iota((tok, tok), 0) == iota((tok, tok), 1)

    def to_row(column):
        return jnp.sum(jnp.where(eye, column, 0.0), axis=0, keepdims=True)

    def to_column(row):
        return jnp.sum(jnp.where(eye, row, 0.0), axis=1, keepdims=True)

    kv[x, 0:tok, :] = k_ref[...]
    kv[x, tok : 2 * tok, :] = v_ref[...]
    bias_row = to_row(b_ref[...].astype(F32))
    kv[x, 2 * tok : 2 * tok + 16, :] = jnp.broadcast_to(bias_row, (16, tok)).astype(BF16)
    hk = (nx // 2) * tok
    tri[...] = (iota((hk, hk), 0) > iota((hk, hk), 1)).astype(BF16)

    pl.semaphore_wait(barrier, nsp - 1 + ny)

    def kv_copy(i):
        peer = lax.rem(x + i, nx)
        return rdma(kv.at[x], kv.at[x], kv_send.at[i], kv_recv.at[x], (z * nx + peer, tp))

    def q_copy(i):
        return rdma(q_ref, qbuf.at[z], q_send.at[i], q_recv.at[z], ((z - i) * nx + x, tp))

    each(1, nx, lambda i: kv_copy(i).start())
    each(1, z + 1, lambda i: q_copy(i).start())

    ids = ids_ref[...]
    rw = rw_ref[...]
    exp_lane = iota((tok, nexp), 1)
    first = ids[:, 0:1] == exp_lane
    second = ids[:, 1:2] == exp_lane
    named = jnp.where(first | second, 1.0, 0.0).astype(BF16)
    earlier = jnp.where(iota((tok, tok), 1) < iota((tok, tok), 0), 1.0, 0.0).astype(BF16)
    rank = dot(earlier, named).astype(BF16)
    spread = jnp.where(iota((nexp, nslot), 1) // cap == iota((nexp, nslot), 0), 1.0, 0.0).astype(BF16)
    weight_hi, weight_lo = halves(jnp.where(first, rw[:, 0:1], 0.0) + jnp.where(second, rw[:, 1:2], 0.0))
    slot_rank = lax.rem(iota((tok, nslot), 1), cap).astype(F32)
    taken = (dot(named, spread) > 0.5) & (dot(rank, spread) == slot_rank)
    taken_f = jnp.where(taken, 1.0, 0.0)
    pt[...] = taken_f.T.astype(BF16)
    w_hi[...] = (taken_f * dot(weight_hi, spread)).astype(BF16)
    w_lo[...] = (taken_f * dot(weight_lo, spread)).astype(BF16)

    def kv_arrive(i):
        xs = lax.rem(x + i, nx)
        rdma(kv.at[xs], kv.at[xs], kv_send.at[i], kv_recv.at[xs], (z * nx + xs, tp)).wait_recv()

    each(1, nx, kv_arrive)

    scale = hd ** (-0.5)

    def attend(q, own):
        logits, fails, parts = [], [], []
        for h in range(2):
            at = range(h * (nx // 2), (h + 1) * (nx // 2))
            keys = jnp.concatenate([kv[i, 0:tok, :] for i in at], axis=0)
            bias = jnp.concatenate([kv[i, 2 * tok : 2 * tok + 1, :] for i in at], axis=1).astype(F32)
            lg = dot_nt(q, keys) * scale + bias
            fail = -(jnp.maximum(lg, 0.0) + jnp.log(1.0 + jnp.exp(-jnp.abs(lg))))
            logits.append(lg + fail)
            if own:
                before = iota((tok, hk), 1) + h * hk < iota((tok, hk), 0) + x * tok
                fail = jnp.where(before, fail, 0.0)
            fails.append(fail)
            parts.append(halves(fail))
        stacked = jnp.concatenate([parts[0][0], parts[1][0], parts[0][1], parts[1][1]], axis=0)
        sums = dot(stacked, tri[...])
        tail0 = sums[0:tok] + sums[2 * tok : 3 * tok]
        tail1 = sums[tok : 2 * tok] + sums[3 * tok : 4 * tok]
        tail0 = tail0 + (tail1[:, 0:1] + fails[1][:, 0:1])
        total = tail0[:, 0:1] + fails[0][:, 0:1]
        acc = jnp.zeros((tok, hd), F32)
        for h, tail in enumerate((tail0, tail1)):
            at = range(h * (nx // 2), (h + 1) * (nx // 2))
            values = jnp.concatenate([kv[i, tok : 2 * tok, :] for i in at], axis=0)
            weights = jnp.exp(logits[h] + tail)
            if own:
                before = iota((tok, hk), 1) + h * hk < iota((tok, hk), 0) + x * tok
                weights = jnp.where(before, weights, 0.0)
            acc = acc + dot(weights.astype(BF16), values)
        return acc, total

    def part_copy(zq):
        return rdma(part_out.at[zq], part_in.at[z], p_send.at[zq], p_recv.at[z], (zq * nx + x, tp))

    def serve(i):
        zq = z + i
        rdma(qbuf.at[zq], qbuf.at[zq], q_send.at[i], q_recv.at[zq], (zq * nx + x, tp)).wait_recv()
        acc, total = attend(qbuf[zq], False)
        part_out[zq, 0:tok, :] = acc.astype(BF16)
        row = to_row(total)
        high, rest = row.astype(BF16), row - row.astype(BF16).astype(F32)
        mid, low = halves(rest)
        at_row = iota((16, tok), 0)
        rows = jnp.where(
            at_row == 0,
            high.astype(F32),
            jnp.where(at_row == 1, mid.astype(F32), jnp.where(at_row == 2, low.astype(F32), 0.0)),
        )
        part_out[zq, tok : tok + 16, :] = rows.astype(BF16)
        part_copy(zq).start()

    each(1, nz - z, serve)
    acc, later = attend(q_ref[...], True)

    def combine(i, carry):
        acc, later = carry
        zs = z - i
        rdma(part_in.at[zs], part_in.at[zs], p_send.at[zs], p_recv.at[zs], (zs * nx + x, tp)).wait_recv()
        summary = part_in[zs, 0:tok, :].astype(F32)
        row = jnp.sum(part_in[zs, tok : tok + 16, :].astype(F32), axis=0, keepdims=True)
        return acc + jnp.exp(later) * summary, later + to_column(row)

    acc, later = lax.fori_loop(1, z + 1, combine, (acc, later))

    def gather_start(buf, send, recv, fsend, frecv):
        mine = buf.at[y, c]

        def to_peer(i):
            off = offset_near(i, ny)
            rdma(mine, mine, send.at[i], recv.at[y], in_column(lax.rem(y + off, ny))).start()

        each(0, ny - 1, to_peer)
        rdma(mine, mine, fsend.at[y], frecv.at[y], partner).start()

    def gather_pass_on(buf, send, recv, fsend, frecv):
        def pass_on(i):
            ys = lax.rem(y + offset_near(i, ny), ny)
            here = buf.at[ys, c]
            rdma(here, here, send.at[i], recv.at[ys], in_column(ys)).wait_recv()
            rdma(here, here, fsend.at[ys], frecv.at[ys], partner).start()

        each(0, ny - 1, pass_on)

        def arrive(ys):
            there = buf.at[ys, 1 - c]
            rdma(there, there, fsend.at[ys], frecv.at[ys], partner).wait_recv()

        each(0, ny, arrive)

    def gather_drain(buf, send, recv, fsend, frecv):
        mine = buf.at[y, c]
        each(0, ny - 1, lambda i: rdma(mine, mine, send.at[i], recv.at[y], partner).wait_send())

        def forwarded(ys):
            here = buf.at[ys, c]
            rdma(here, here, fsend.at[ys], frecv.at[ys], partner).wait_send()

        each(0, ny, forwarded)

    a_args = (abuf, a_send, a_recv, af_send, af_recv)
    abuf[y, c] = acc.astype(BF16)
    gather_start(*a_args)
    gather_pass_on(*a_args)
    loads[0].wait()
    projected = jnp.zeros((tok, feat), F32)
    for i in range(ny):
        heads = jnp.concatenate([abuf[i, 0], abuf[i, 1]], axis=1)
        projected = projected + dot(heads, wo[i * 2 * hd : (i + 1) * 2 * hd, :])
    mixed = (stream_ref[...].astype(F32) + projected).astype(BF16)
    mixed_ref[...] = mixed

    snd[...] = dot(pt[...], mixed).astype(BF16).reshape(nsp, per_dest, feat)

    def dispatch(i):
        to = lax.rem(sp + i, nsp)
        return rdma(snd.at[to], arr.at[sp], d_send.at[i], d_recv.at[sp], (to, tp))

    each(1, nsp, lambda i: dispatch(i).start())
    arr[sp] = snd[sp]

    gain = gain_ref[...]

    def products(rows, lhs_of, gate_w, up_w):
        value = rows.astype(F32)
        squares = jnp.sum(value * value, axis=1, keepdims=True)
        lhs = lhs_of((value * gain).astype(BF16))
        gate = dot(lhs, gate_w).astype(BF16)
        up = dot(lhs, up_w).astype(BF16)
        return gate, up, two_lanes(squares)

    def two_lanes(column):
        high, low = halves(column)
        lane = iota((column.shape[0], 128), 1)
        return jnp.where(
            lane == 0, high.astype(F32), jnp.where(lane == 1, low.astype(F32), 0.0)
        ).astype(BF16)

    def laid(ref, lo, value):
        ref[:, :, lo : lo + value.shape[1]] = value.reshape(ref.shape[0], ref.shape[1], value.shape[1])

    def added(mine, theirs):
        both = mine.astype(F32) + theirs.astype(F32)
        squares = both[:, 2 * ffe : 2 * ffe + 1] + both[:, 2 * ffe + 1 : 2 * ffe + 2]
        return both[:, 0 : 2 * ffe].astype(BF16), two_lanes(squares)

    def activated(total):
        squares = total[:, 2 * ffe : 2 * ffe + 1] + total[:, 2 * ffe + 1 : 2 * ffe + 2]
        inv = lax.rsqrt(squares / width + EPS)
        gate, up = total[:, 0:ffe] * inv, total[:, ffe : 2 * ffe] * inv
        return (gate * jax.nn.sigmoid(gate) * up).astype(BF16)

    loads[1].wait()
    loads[2].wait()
    gate, up, squares = products(mixed, lambda a: a, sg[...], su[...])
    laid(spart, 0, gate)
    laid(spart, ffe, up)
    laid(spart, 2 * ffe, squares)
    ny2 = ny // 2

    def spre_copy(i):
        yy = 2 * i + 1 - c
        return rdma(spart.at[yy], spre.at[i], spre_send.at[i], spre_recv.at[i], partner)

    each(0, ny2, lambda i: spre_copy(i).start())

    def srs_copy(i):
        yy = 2 * i + c
        return rdma(sred.at[i], srs_in.at[y], srs_send.at[i], srs_recv.at[y], in_column(yy))

    def shared_add(i):
        yy = 2 * i + c
        rdma(spre.at[i], spre.at[i], spre_send.at[i], spre_recv.at[i], partner).wait_recv()
        sums, squares = added(spart[yy], spre[i])
        sred[i, :, 0 : 2 * ffe] = sums
        sred[i, :, 2 * ffe : 2 * ffe + 128] = squares

        @pl.when(yy != y)
        def _():
            srs_copy(i).start()

    each(0, ny2, shared_add)

    def arrive(i):
        src = lax.rem(sp + i, nsp)
        rdma(arr.at[src], arr.at[src], d_send.at[i], d_recv.at[src], (src, tp)).wait_recv()

    each(1, nsp, arrive)
    loads[3].wait()
    loads[4].wait()

    def by_expert(a):
        zero = jnp.zeros_like(a)
        mine = lax.rem(iota(a.shape, 0), per_dest) < cap
        return jnp.concatenate([jnp.where(mine, a, zero), jnp.where(mine, zero, a)], axis=1)

    gate, up, squares = products(arr[...].reshape(nslot, feat), by_expert, wg[...], wu[...])
    laid(part, 0, gate)
    laid(part, ffe, up)
    laid(part, 2 * ffe, squares)

    def pre_copy(i):
        yy = lax.rem(y + offset_near(ny - 2 - i, ny), ny)
        yy = jnp.where(i == ny - 1, y, yy)
        return rdma(part.at[yy * 2 + 1 - c], pre.at[yy], pre_send.at[i], pre_recv.at[yy], partner)

    each(0, ny, lambda i: pre_copy(i).start())

    def rs_copy(i):
        yy = lax.rem(y + offset_near(ny - 2 - i, ny), ny)
        return rdma(red.at[yy], rs_in.at[y], rs_send.at[i], rs_recv.at[y], in_column(yy))

    def pair_add(yy):
        rdma(pre.at[yy], pre.at[yy], pre_send.at[0], pre_recv.at[yy], partner).wait_recv()
        sums, squares = added(part[yy * 2 + c], pre[yy])
        red[yy, :, 0 : 2 * ffe] = sums
        red[yy, :, 2 * ffe : 2 * ffe + 128] = squares

    def pair_step(i):
        pair_add(lax.rem(y + offset_near(ny - 2 - i, ny), ny))
        rs_copy(i).start()

    each(0, ny - 1, pair_step)
    pair_add(y)

    sh_args = (shbuf, sh_send, sh_recv, shf_send, shf_recv)
    owner = lax.rem(y, 2) == c

    @pl.when(owner)
    def _():
        def add_in(i, total):
            ys = lax.rem(y + offset_near(i, ny), ny)
            rdma(srs_in.at[ys], srs_in.at[ys], srs_send.at[0], srs_recv.at[ys], partner).wait_recv()
            return total + srs_in[ys].astype(F32)

        total = lax.fori_loop(0, ny - 1, add_in, sred[y // 2].astype(F32))
        shbuf[y] = activated(total)

        def to_peer(i):
            off = offset_near(i, ny)
            rdma(
                shbuf.at[y], shbuf.at[y], sh_send.at[i], sh_recv.at[y], in_column(lax.rem(y + off, ny))
            ).start()

        each(0, ny - 1, to_peer)
        rdma(shbuf.at[y], shbuf.at[y], shf_send.at[y // 2], shf_recv.at[y], partner).start()

    def add_routed(i, total):
        ys = lax.rem(y + offset_near(i, ny), ny)
        rdma(rs_in.at[ys], rs_in.at[ys], rs_send.at[0], rs_recv.at[ys], partner).wait_recv()
        return total + rs_in[ys].astype(F32)

    total = lax.fori_loop(0, ny - 1, add_routed, red[y].astype(F32))
    hbuf[y, c] = activated(total)
    h_args = (hbuf, h_send, h_recv, hf_send, hf_recv)
    gather_start(*h_args)

    def shared_on(i):
        yy = 2 * i + c

        @pl.when(yy != y)
        def _():
            rdma(shbuf.at[yy], shbuf.at[yy], sh_send.at[0], sh_recv.at[yy], partner).wait_recv()
            rdma(shbuf.at[yy], shbuf.at[yy], shf_send.at[i], shf_recv.at[yy], partner).start()

    each(0, ny2, shared_on)
    gather_pass_on(*h_args)

    def expert_rows():
        rows = hbuf[...].reshape(nslot, ffe)
        return by_expert(rows)

    loads[6].wait()
    ret_out[...] = dot(expert_rows(), wd[...]).astype(BF16).reshape(nsp, per_dest, feat)

    def give_back(i):
        to = lax.rem(sp + i, nsp)
        return rdma(ret_out.at[to], ret_in.at[sp], r_send.at[i], r_recv.at[sp], (to, tp))

    each(1, nsp, lambda i: give_back(i).start())
    ret_in[sp] = ret_out[sp]

    def shared_arrive(i):
        yy = 2 * i + 1 - c
        rdma(shbuf.at[yy], shbuf.at[yy], shf_send.at[i], shf_recv.at[yy], partner).wait_recv()

    each(0, ny2, shared_arrive)
    loads[5].wait()
    base = mixed_ref[...].astype(F32) + dot(shbuf[...].reshape(tok, ffe), sd[...])

    each(1, nx, lambda i: kv_copy(i).wait_send())
    each(1, z + 1, lambda i: q_copy(i).wait_send())
    each(1, nz - z, lambda i: part_copy(z + i).wait_send())
    gather_drain(*a_args)
    each(1, nsp, lambda i: dispatch(i).wait_send())
    each(0, ny2, lambda i: spre_copy(i).wait_send())

    def srs_drain(i):
        @pl.when(2 * i + c != y)
        def _():
            srs_copy(i).wait_send()

    each(0, ny2, srs_drain)
    each(0, ny, lambda i: pre_copy(i).wait_send())
    each(0, ny - 1, lambda i: rs_copy(i).wait_send())
    gather_drain(*h_args)

    @pl.when(owner)
    def _():
        each(
            0,
            ny - 1,
            lambda i: rdma(shbuf.at[y], shbuf.at[y], sh_send.at[i], sh_recv.at[y], partner).wait_send(),
        )

    def shared_forwarded(i):
        yy = 2 * i + c
        rdma(shbuf.at[yy], shbuf.at[yy], shf_send.at[i], shf_recv.at[yy], partner).wait_send()

    each(0, ny2, shared_forwarded)

    def returned(i):
        src = lax.rem(sp + i, nsp)
        rdma(ret_in.at[src], ret_in.at[src], r_send.at[i], r_recv.at[src], (src, tp)).wait_recv()

    each(1, nsp, returned)
    rows = ret_in[...].reshape(nslot, feat)
    out_ref[...] = (base + (dot(w_hi[...], rows) + dot(w_lo[...], rows))).astype(BF16)
    each(1, nsp, lambda i: give_back(i).wait_send())


def body(
    nx,
    queries,
    key_rows,
    value_rows,
    break_bias,
    stream,
    out_proj,
    norm_gain,
    expert_ids,
    route_weights,
    gate_proj,
    up_proj,
    down_proj,
    shared_gate,
    shared_up,
    shared_down,
):
    nsp, ntp = lax.axis_size("sp"), lax.axis_size("tp")
    nz, ny = nsp // nx, ntp // 2
    tok, hd = queries.shape
    feat = stream.shape[1]
    experts_local, _, ffe = gate_proj.shape
    ffs = shared_gate.shape[1]
    cap = 2 * expert_ids.shape[1] * tok // (experts_local * nsp)
    per_dest = experts_local * cap
    chunk = nsp * per_dest // ntp
    srows = tok // ny
    wide = 2 * ffe + 128
    hk = (nx // 2) * tok

    def vm(*shape):
        return pltpu.VMEM(shape, BF16)

    def sems(*counts):
        return [pltpu.SemaphoreType.DMA((n,)) for n in counts]

    scratch = [
        vm(*out_proj.shape),
        vm(experts_local * feat, ffe),
        vm(experts_local * feat, ffe),
        vm(experts_local * ffe, feat),
        vm(feat, ffs),
        vm(feat, ffs),
        vm(ffs, feat),
        vm(nx, 2 * tok + 16, hd),
        vm(nz, tok, hd),
        vm(nz, tok + 16, hd),
        vm(nz, tok + 16, hd),
        vm(hk, hk),
        vm(ny, 2, tok, hd),
        vm(nsp * per_dest, tok),
        vm(tok, nsp * per_dest),
        vm(tok, nsp * per_dest),
        vm(tok, feat),
        vm(nsp, per_dest, feat),
        vm(nsp, per_dest, feat),
        vm(ntp, chunk, wide),
        vm(ny, chunk, wide),
        vm(ny, chunk, wide),
        vm(ny, chunk, wide),
        vm(ny, srows, wide),
        vm(ny // 2, srows, wide),
        vm(ny // 2, srows, wide),
        vm(ny, srows, wide),
        vm(ny, 2, chunk, ffe),
        vm(ny, srows, ffs),
        vm(nsp, per_dest, feat),
        vm(nsp, per_dest, feat),
        *sems(7, nx, nx, nz, nz, nz, nz, ny, ny, ny, ny, nsp, nsp, ny, ny, ny, ny),
        *sems(ny // 2, ny // 2, ny // 2, ny, ny, ny, ny, ny, ny, ny, ny // 2, ny, nsp, nsp),
    ]
    small = pl.BlockSpec(memory_space=pltpu.VMEM)
    large = pl.BlockSpec(memory_space=pl.ANY)
    return pl.pallas_call(
        functools.partial(layer_kernel, (nz, nx, ny)),
        out_shape=jax.ShapeDtypeStruct((tok, feat), BF16),
        in_specs=[small] * 8 + [large] * 7,
        out_specs=small,
        scratch_shapes=scratch,
        compiler_params=pltpu.CompilerParams(
            collective_id=0, has_side_effects=True, vmem_limit_bytes=60 * 1024 * 1024
        ),
    )(
        queries,
        key_rows,
        value_rows,
        break_bias,
        stream,
        norm_gain.reshape(1, feat),
        expert_ids,
        route_weights,
        out_proj,
        gate_proj.reshape(experts_local * feat, ffe),
        up_proj.reshape(experts_local * feat, ffe),
        down_proj.reshape(experts_local * ffe, feat),
        shared_gate,
        shared_up,
        shared_down,
    )


def solution(mesh, nx=NX):
    in_specs = (
        P("sp", "tp"),
        P("sp", "tp"),
        P("sp", "tp"),
        P("sp", "tp"),
        P("sp", "tp"),
        P(None, "tp"),
        P("tp"),
        P("sp", None),
        P("sp", None),
        P("sp", "tp", None),
        P("sp", "tp", None),
        P("sp", None, "tp"),
        P("tp", None),
        P("tp", None),
        P(None, "tp"),
    )
    return jax.shard_map(
        functools.partial(body, nx), mesh=mesh, in_specs=in_specs, out_specs=P("sp", "tp"), check_vma=False
    )
```

time: 441 us -> 90.7 us (0.21)
  other arithmetic: 169 us -> 0 us
  waiting for transfers between devices: 161 us -> 0 us
  Pallas kernels: 0 us -> 86.1 us
  starting transfers between devices: 33.2 us -> 0 us
  local copies, waits for them, and re-layouts: 25.3 us -> 4.34 us
  matrix products: 19.2 us -> 0 us
  blocking collectives: 15.8 us -> 0 us
  between operations: 13.8 us -> 0.01 us
    another operation x13 -> x0, other arithmetic: 161 us -> none
    all_gather x1 -> x0, waiting for transfers between devices: 87.4 us -> none  [sent_together(): filled = lax.all_gather(both, axis, axis=dim, tiled=True)]
    pallas_call x0 -> x1, Pallas kernels: none -> 86.1 us  [body(): pl.pallas_call(functools.partial(layer_kernel, (nz, nx, ny)), out_shape=j...]
    all_to_all x6 -> x0, waiting for transfers between devices: 73.4 us -> none  [the longest x2 30.5 us: summed_on_arrival(): lax.all_to_all(blocks, axis, split_axis=0, concat_axis=0, tiled=True)]
    all_to_all x6 -> x0, starting transfers between devices: 33.2 us -> none  [the longest x2 14.8 us: from_everyone(): return lax.all_to_all(copies, axis, split_axis=0, concat_axis=0, tiled=True)]
    dot_general x16 -> x0, matrix products: 19.2 us -> none  [the longest x4 9.66 us: block_terms(): summary = jnp.einsum('hts,shd->thd', weights, value_heads)]
    all_gather x1 -> x0, blocking collectives: 15.8 us -> none  [gather_packed(): lines, at, outs = (lax.all_gather(line, axis), 0, [])]
    another operation x13 -> x0, local copies, waits for them, and re-layouts: 4.56 us -> none
  transfers between devices with their start and end apart: 7 -> 0, of which waited for: 7 -> 0; matrix products, arithmetic and copies ran while one was open for 2% -> 0% of each run, Pallas kernels for 0% -> 0%
where the time goes in v1:
time: 90.7 us; the launch traced here: 90.5 us
  Pallas kernels  86.1 us (95%)
  local copies, waits for them, and re-layouts  4.34 us (5%)
    pallas_call x1, Pallas kernels, body(): pl.pallas_call(functools.partial(layer_kernel, (nz, nx, ny)), out_shape=j...  86.1 us
    unnamed x10, local copies, waits for them, and re-layouts  4.34 us

profile of v1, /device:TPU:1, one launch (start us, length us, event | category | flops | bytes accessed | tf_op | source)
XLA Modules:
  0.0 90.5 jit_solution(14109620160393300893)
XLA Ops:
  0.0 0.0 copy-start.2
  0.0 0.7 copy-done.2
  0.7 0.0 copy-start
  0.7 0.7 copy.16.b_ref
  1.4 0.0 copy-done
  1.4 0.0 copy-start.1
  1.4 0.7 copy.17.ids_ref
  2.1 0.0 copy-done.1
  2.1 0.7 copy.18.rw_ref
  2.9 86.1 %shard_map.145 = bf16[128,256]{1,0:T(8,128)(2,1)} custom-call(bf16[128,128]{1,0:T(8,128)(2,1)} %q_ref.1, bf16[128,128]{1,0:T(8,128)(2,1)} %k_ref.1, bf16[128,128]{1,0:T(8,128)(2,1)} %v_ref.1, bf16[128,1]{1,0:T(8,128)(2,1)} %copy.16.b_ref, bf16[128,256]{1,0:T(8,128)(2,1)} %stream_ref.1, f32[1,256]{1,0:T(1,128)} %bitcast.7, s32[128,2]{1,0:T(8,128)} %copy.17.ids_ref, ...), custom_call_target="tpu_custom_call" | custom-call | tf_op jit(solution)/shard_map/pallas_call | solution.py:630
  89.0 1.5 %copy.20 = bf16[128,256]{1,0:T(8,128)(2,1)} copy(bf16[128,256]{1,0:T(8,128)(2,1)} %shard_map.145) | data formatting | bytes 131072
Async XLA Ops:
  0.0 0.7 copy-start.2
  0.7 0.7 copy-start
  1.4 0.7 copy-start.1

commit v2 on v1

--- a/solution.py
+++ b/solution.py
@@ -51,14 +51,14 @@
 
 def layer_kernel(
     sizes,
-    q_ref,
-    k_ref,
-    v_ref,
-    b_ref,
-    stream_ref,
-    gain_ref,
-    ids_ref,
-    rw_ref,
+    q_hbm,
+    k_hbm,
+    v_hbm,
+    bias_hbm,
+    stream_hbm,
+    gain_hbm,
+    ids_hbm,
+    rw_hbm,
     wo_hbm,
     wg_hbm,
     wu_hbm,
@@ -67,6 +67,12 @@
     su_hbm,
     sd_hbm,
     out_ref,
+    q_ref,
+    bias_ref,
+    stream_ref,
+    gain_ref,
+    ids_ref,
+    rw_ref,
     wo,
     wg,
     wu,
@@ -89,7 +95,9 @@
     part,
     pre,
     red,
-    rs_in,
+    hub_in,
+    hub_out,
+    own_in,
     spart,
     spre,
     sred,
@@ -113,8 +121,10 @@
     d_recv,
     pre_send,
     pre_recv,
-    rs_send,
-    rs_recv,
+    l1_send,
+    l1_recv,
+    l2_send,
+    l2_recv,
     spre_send,
     spre_recv,
     srs_send,
@@ -148,12 +158,8 @@
     def in_column(yy):
         return (sp, yy * 2 + c)
 
-    loads = [
-        pltpu.make_async_copy(src, dst, load_sem.at[i])
-        for i, (src, dst) in enumerate(
-            [(wo_hbm, wo), (sg_hbm, sg), (su_hbm, su), (wg_hbm, wg), (wu_hbm, wu), (sd_hbm, sd), (wd_hbm, wd)]
-        )
-    ]
+    def load(i, src, dst):
+        return pltpu.make_async_copy(src, dst, load_sem.at[i])
 
     barrier = pltpu.get_barrier_semaphore()
 
@@ -168,6 +174,28 @@
     each(1, nsp, greet_sp)
     each(1, ny, greet_tp)
     pl.semaphore_signal(barrier, inc=1, device_id=partner, device_id_type=MESH)
+    loads = [
+        load(i, src, dst)
+        for i, (src, dst) in enumerate(
+            [
+                (bias_hbm, bias_ref),
+                (k_hbm, kv.at[x, 0:tok]),
+                (v_hbm, kv.at[x, tok : 2 * tok]),
+                (q_hbm, q_ref),
+                (ids_hbm, ids_ref),
+                (rw_hbm, rw_ref),
+                (stream_hbm, stream_ref),
+                (gain_hbm, gain_ref),
+                (wo_hbm, wo),
+                (sg_hbm, sg),
+                (su_hbm, su),
+                (wg_hbm, wg),
+                (wu_hbm, wu),
+                (wd_hbm, wd),
+                (sd_hbm, sd),
+            ]
+        )
+    ]
     for copy in loads:
         copy.start()
 
@@ -179,12 +207,12 @@
     def to_column(row):
         return jnp.sum(jnp.where(eye, row, 0.0), axis=1, keepdims=True)
 
-    kv[x, 0:tok, :] = k_ref[...]
-    kv[x, tok : 2 * tok, :] = v_ref[...]
-    bias_row = to_row(b_ref[...].astype(F32))
-    kv[x, 2 * tok : 2 * tok + 16, :] = jnp.broadcast_to(bias_row, (16, tok)).astype(BF16)
+    loads[0].wait()
+    kv[x, 2 * tok : 2 * tok + 16, :] = jnp.broadcast_to(bias_ref[...].astype(F32), (16, tok)).astype(BF16)
     hk = (nx // 2) * tok
     tri[...] = (iota((hk, hk), 0) > iota((hk, hk), 1)).astype(BF16)
+    for i in (1, 2, 3):
+        loads[i].wait()
 
     pl.semaphore_wait(barrier, nsp - 1 + ny)
 
@@ -198,16 +226,20 @@
     each(1, nx, lambda i: kv_copy(i).start())
     each(1, z + 1, lambda i: q_copy(i).start())
 
-    ids = ids_ref[...]
-    rw = rw_ref[...]
-    exp_lane = iota((tok, nexp), 1)
-    first = ids[:, 0:1] == exp_lane
-    second = ids[:, 1:2] == exp_lane
+    loads[4].wait()
+    loads[5].wait()
+    exp_lane = iota((tok, nexp), 1).astype(F32)
+
+    def columns(ref):
+        return [to_column(ref[i : i + 1, :].astype(F32)) for i in range(2)]
+
+    ids, rw = columns(ids_ref), columns(rw_ref)
+    first, second = ids[0] == exp_lane, ids[1] == exp_lane
     named = jnp.where(first | second, 1.0, 0.0).astype(BF16)
     earlier = jnp.where(iota((tok, tok), 1) < iota((tok, tok), 0), 1.0, 0.0).astype(BF16)
     rank = dot(earlier, named).astype(BF16)
     spread = jnp.where(iota((nexp, nslot), 1) // cap == iota((nexp, nslot), 0), 1.0, 0.0).astype(BF16)
-    weight_hi, weight_lo = halves(jnp.where(first, rw[:, 0:1], 0.0) + jnp.where(second, rw[:, 1:2], 0.0))
+    weight_hi, weight_lo = halves(jnp.where(first, rw[0], 0.0) + jnp.where(second, rw[1], 0.0))
     slot_rank = lax.rem(iota((tok, nslot), 1), cap).astype(F32)
     taken = (dot(named, spread) > 0.5) & (dot(rank, spread) == slot_rank)
     taken_f = jnp.where(taken, 1.0, 0.0)
@@ -257,6 +289,13 @@
     def part_copy(zq):
         return rdma(part_out.at[zq], part_in.at[z], p_send.at[zq], p_recv.at[z], (zq * nx + x, tp))
 
+    def serve_far_first(i):
+        off = offset_near(nz - 2 - i, nz)
+
+        @pl.when(z + off < nz)
+        def _():
+            serve(off)
+
     def serve(i):
         zq = z + i
         rdma(qbuf.at[zq], qbuf.at[zq], q_send.at[i], q_recv.at[zq], (zq * nx + x, tp)).wait_recv()
@@ -274,7 +313,7 @@
         part_out[zq, tok : tok + 16, :] = rows.astype(BF16)
         part_copy(zq).start()
 
-    each(1, nz - z, serve)
+    each(0, nz - 1, serve_far_first)
     acc, later = attend(q_ref[...], True)
 
     def combine(i, carry):
@@ -287,62 +326,72 @@
 
     acc, later = lax.fori_loop(1, z + 1, combine, (acc, later))
 
-    def gather_start(buf, send, recv, fsend, frecv):
-        mine = buf.at[y, c]
-
-        def to_peer(i):
-            off = offset_near(i, ny)
-            rdma(mine, mine, send.at[i], recv.at[y], in_column(lax.rem(y + off, ny))).start()
-
-        each(0, ny - 1, to_peer)
-        rdma(mine, mine, fsend.at[y], frecv.at[y], partner).start()
-
-    def gather_pass_on(buf, send, recv, fsend, frecv):
-        def pass_on(i):
-            ys = lax.rem(y + offset_near(i, ny), ny)
-            here = buf.at[ys, c]
-            rdma(here, here, send.at[i], recv.at[ys], in_column(ys)).wait_recv()
-            rdma(here, here, fsend.at[ys], frecv.at[ys], partner).start()
-
-        each(0, ny - 1, pass_on)
-
-        def arrive(ys):
-            there = buf.at[ys, 1 - c]
-            rdma(there, there, fsend.at[ys], frecv.at[ys], partner).wait_recv()
-
-        each(0, ny, arrive)
-
-    def gather_drain(buf, send, recv, fsend, frecv):
-        mine = buf.at[y, c]
-        each(0, ny - 1, lambda i: rdma(mine, mine, send.at[i], recv.at[y], partner).wait_send())
-
-        def forwarded(ys):
-            here = buf.at[ys, c]
-            rdma(here, here, fsend.at[ys], frecv.at[ys], partner).wait_send()
-
-        each(0, ny, forwarded)
-
-    a_args = (abuf, a_send, a_recv, af_send, af_recv)
-    abuf[y, c] = acc.astype(BF16)
-    gather_start(*a_args)
-    gather_pass_on(*a_args)
-    loads[0].wait()
+    far_first = (4, 3, 5, 2, 6, 1, 7)
+
+    def gather(buf, send, recv, fsend, frecv):
+        def block_copy(k, block, off):
+            here = buf.at[c, block]
+            return rdma(here, here, send.at[k], recv.at[block], in_column(lax.rem(y + off, ny)))
+
+        def across(block):
+            here = buf.at[c, block]
+            return rdma(here, here, fsend.at[block], frecv.at[block], partner)
+
+        def start():
+            for k, off in enumerate(far_first):
+                block_copy(k, y, off).start()
+            across(y).start()
+
+        def pass_on():
+            for k, off in enumerate(far_first):
+                block = lax.rem(y + ny - off, ny)
+                block_copy(k, block, off).wait_recv()
+                across(block).start()
+
+        def finish():
+            def arrive(block):
+                there = buf.at[1 - c, block]
+                rdma(there, there, fsend.at[block], frecv.at[block], partner).wait_recv()
+
+            each(0, ny, arrive)
+
+        def drain():
+            for k, off in enumerate(far_first):
+                block_copy(k, y, off).wait_send()
+            each(0, ny, lambda block: across(block).wait_send())
+
+        return start, pass_on, finish, drain
+
+    abuf[c, y] = acc.astype(BF16)
+    a_start, a_pass, a_finish, a_drain = gather(abuf, a_send, a_recv, af_send, af_recv)
+    a_start()
+    a_pass()
+    a_finish()
+    loads[8].wait()
+    loads[6].wait()
     projected = jnp.zeros((tok, feat), F32)
     for i in range(ny):
-        heads = jnp.concatenate([abuf[i, 0], abuf[i, 1]], axis=1)
+        heads = jnp.concatenate([abuf[0, i], abuf[1, i]], axis=1)
         projected = projected + dot(heads, wo[i * 2 * hd : (i + 1) * 2 * hd, :])
     mixed = (stream_ref[...].astype(F32) + projected).astype(BF16)
     mixed_ref[...] = mixed
 
     snd[...] = dot(pt[...], mixed).astype(BF16).reshape(nsp, per_dest, feat)
 
+    def block_at(i, sign):
+        rank = i // nx
+        dz = jnp.where(rank == 0, 0, offset_near(rank - 1, nz))
+        dx = lax.rem(i, nx)
+        return lax.rem(z + sign * dz + nz, nz) * nx + lax.rem(x + sign * dx + nx, nx)
+
     def dispatch(i):
-        to = lax.rem(sp + i, nsp)
-        return rdma(snd.at[to], arr.at[sp], d_send.at[i], d_recv.at[sp], (to, tp))
+        to = block_at(i, -1)
+        return rdma(snd.at[to], arr.at[i], d_send.at[i], d_recv.at[i], (to, tp))
 
     each(1, nsp, lambda i: dispatch(i).start())
-    arr[sp] = snd[sp]
-
+    arr[0] = snd[sp]
+
+    loads[7].wait()
     gain = gain_ref[...]
 
     def products(rows, lhs_of, gate_w, up_w):
@@ -363,10 +412,9 @@
     def laid(ref, lo, value):
         ref[:, :, lo : lo + value.shape[1]] = value.reshape(ref.shape[0], ref.shape[1], value.shape[1])
 
-    def added(mine, theirs):
-        both = mine.astype(F32) + theirs.astype(F32)
-        squares = both[:, 2 * ffe : 2 * ffe + 1] + both[:, 2 * ffe + 1 : 2 * ffe + 2]
-        return both[:, 0 : 2 * ffe].astype(BF16), two_lanes(squares)
+    def packed(total):
+        squares = total[:, 2 * ffe : 2 * ffe + 1] + total[:, 2 * ffe + 1 : 2 * ffe + 2]
+        return total[:, 0 : 2 * ffe].astype(BF16), two_lanes(squares)
 
     def activated(total):
         squares = total[:, 2 * ffe : 2 * ffe + 1] + total[:, 2 * ffe + 1 : 2 * ffe + 2]
@@ -374,8 +422,8 @@
         gate, up = total[:, 0:ffe] * inv, total[:, ffe : 2 * ffe] * inv
         return (gate * jax.nn.sigmoid(gate) * up).astype(BF16)
 
-    loads[1].wait()
-    loads[2].wait()
+    loads[9].wait()
+    loads[10].wait()
     gate, up, squares = products(mixed, lambda a: a, sg[...], su[...])
     laid(spart, 0, gate)
     laid(spart, ffe, up)
@@ -395,7 +443,7 @@
     def shared_add(i):
         yy = 2 * i + c
         rdma(spre.at[i], spre.at[i], spre_send.at[i], spre_recv.at[i], partner).wait_recv()
-        sums, squares = added(spart[yy], spre[i])
+        sums, squares = packed(spart[yy].astype(F32) + spre[i].astype(F32))
         sred[i, :, 0 : 2 * ffe] = sums
         sred[i, :, 2 * ffe : 2 * ffe + 128] = squares
 
@@ -405,50 +453,101 @@
 
     each(0, ny2, shared_add)
 
-    def arrive(i):
-        src = lax.rem(sp + i, nsp)
-        rdma(arr.at[src], arr.at[src], d_send.at[i], d_recv.at[src], (src, tp)).wait_recv()
-
-    each(1, nsp, arrive)
-    loads[3].wait()
-    loads[4].wait()
+    npos, rows_g, chunk = nsp // 2, nslot // 2, part.shape[3]
 
     def by_expert(a):
         zero = jnp.zeros_like(a)
         mine = lax.rem(iota(a.shape, 0), per_dest) < cap
         return jnp.concatenate([jnp.where(mine, a, zero), jnp.where(mine, zero, a)], axis=1)
 
-    gate, up, squares = products(arr[...].reshape(nslot, feat), by_expert, wg[...], wu[...])
-    laid(part, 0, gate)
-    laid(part, ffe, up)
-    laid(part, 2 * ffe, squares)
-
-    def pre_copy(i):
-        yy = lax.rem(y + offset_near(ny - 2 - i, ny), ny)
-        yy = jnp.where(i == ny - 1, y, yy)
-        return rdma(part.at[yy * 2 + 1 - c], pre.at[yy], pre_send.at[i], pre_recv.at[yy], partner)
-
-    each(0, ny, lambda i: pre_copy(i).start())
-
-    def rs_copy(i):
-        yy = lax.rem(y + offset_near(ny - 2 - i, ny), ny)
-        return rdma(red.at[yy], rs_in.at[y], rs_send.at[i], rs_recv.at[y], in_column(yy))
-
-    def pair_add(yy):
-        rdma(pre.at[yy], pre.at[yy], pre_send.at[0], pre_recv.at[yy], partner).wait_recv()
-        sums, squares = added(part[yy * 2 + c], pre[yy])
-        red[yy, :, 0 : 2 * ffe] = sums
-        red[yy, :, 2 * ffe : 2 * ffe + 128] = squares
-
-    def pair_step(i):
-        pair_add(lax.rem(y + offset_near(ny - 2 - i, ny), ny))
-        rs_copy(i).start()
-
-    each(0, ny - 1, pair_step)
-    pair_add(y)
-
-    sh_args = (shbuf, sh_send, sh_recv, shf_send, shf_recv)
+    def pre_copy(g):
+        return rdma(part.at[g, 1 - c], pre.at[g], pre_send.at[g], pre_recv.at[g], partner)
+
+    def arrivals(g):
+        def arrive(i):
+            rdma(arr.at[i], arr.at[i], d_send.at[i], d_recv.at[i], partner).wait_recv()
+
+        each(max(1, g * npos), (g + 1) * npos, arrive)
+
+    def experts(g):
+        rows = arr[g * npos : (g + 1) * npos].reshape(rows_g, feat)
+        gate, up, squares = products(rows, by_expert, wg[...], wu[...])
+        for lo, value in ((0, gate), (ffe, up), (2 * ffe, squares)):
+            part[g, :, :, :, lo : lo + value.shape[1]] = value.reshape(2, ny, chunk, value.shape[1])
+        pre_copy(g).start()
+
+    def l1_copy(g, r):
+        if r == 4:
+            side = lax.rem(y, 2)
+            hub, k = jnp.where(side == 0, 3, 5), 2
+        else:
+            side = 0 if r < 4 else 1
+            hub, k = (r - 1, r - 2) if r < 4 else (r + 1, ny - r - 2)
+        return rdma(
+            red.at[g, lax.rem(y + r, ny)],
+            hub_in.at[g, side, k],
+            l1_send.at[g, r],
+            l1_recv.at[g, side, k],
+            in_column(lax.rem(y + hub, ny)),
+        )
+
+    def pair_add(g):
+        pre_copy(g).wait_recv()
+        both = part[g, c].astype(F32) + pre[g].astype(F32)
+        sums, squares = packed(both.reshape(ny * chunk, both.shape[-1]))
+        red[g, :, :, 0 : 2 * ffe] = sums.reshape(ny, chunk, 2 * ffe)
+        red[g, :, :, 2 * ffe : 2 * ffe + 128] = squares.reshape(ny, chunk, 128)
+        for r in (4, 3, 5, 2, 6):
+            l1_copy(g, r).start()
+
+    def l2_copy(g, side):
+        to = lax.rem(y + (1 if side == 0 else ny - 1), ny)
+        return rdma(hub_out.at[g, side], own_in.at[g, side], l2_send.at[g, side], l2_recv.at[g, side], in_column(to))
+
+    def hub(g):
+        for side in range(2):
+            def add_in(k, total):
+                here = hub_in.at[g, side, k]
+                rdma(here, here, l1_send.at[g, 2], l1_recv.at[g, side, k], partner).wait_recv()
+                return total + hub_in[g, side, k].astype(F32)
+
+            odd = lax.rem(y, 2)
+            mine = red[g, lax.rem(y + (1 if side == 0 else ny - 1), ny)].astype(F32)
+            total = lax.fori_loop(0, 2 + odd if side == 0 else 3 - odd, add_in, mine)
+            sums, squares = packed(total)
+            hub_out[g, side, :, 0 : 2 * ffe] = sums
+            hub_out[g, side, :, 2 * ffe : 2 * ffe + 128] = squares
+            l2_copy(g, side).start()
+
+    gathers = [gather(hbuf.at[g], h_send.at[g], h_recv.at[g], hf_send.at[g], hf_recv.at[g]) for g in range(2)]
+
+    def own(g):
+        total = red[g, y].astype(F32)
+        for side in range(2):
+            here = own_in.at[g, side]
+            rdma(here, here, l2_send.at[g, side], l2_recv.at[g, side], partner).wait_recv()
+            total = total + own_in[g, side].astype(F32)
+        hbuf[g, c, y] = activated(total)
+        gathers[g][0]()
+
+    def give_back(i):
+        to = block_at(i, 1)
+        return rdma(ret_out.at[i], ret_in.at[sp], r_send.at[i], r_recv.at[i], (to, tp))
+
+    def down(g):
+        rows = by_expert(hbuf[g].reshape(rows_g, ffe))
+        ret_out[g * npos : (g + 1) * npos] = dot(rows, wd[...]).astype(BF16).reshape(npos, per_dest, feat)
+        each(max(1, g * npos), (g + 1) * npos, lambda i: give_back(i).start())
+        if g == 0:
+            ret_in[sp] = ret_out[0]
+
     owner = lax.rem(y, 2) == c
+
+    arrivals(0)
+    loads[11].wait()
+    loads[12].wait()
+    experts(0)
+    pair_add(0)
 
     @pl.when(owner)
     def _():
@@ -469,16 +568,14 @@
         each(0, ny - 1, to_peer)
         rdma(shbuf.at[y], shbuf.at[y], shf_send.at[y // 2], shf_recv.at[y], partner).start()
 
-    def add_routed(i, total):
-        ys = lax.rem(y + offset_near(i, ny), ny)
-        rdma(rs_in.at[ys], rs_in.at[ys], rs_send.at[0], rs_recv.at[ys], partner).wait_recv()
-        return total + rs_in[ys].astype(F32)
-
-    total = lax.fori_loop(0, ny - 1, add_routed, red[y].astype(F32))
-    hbuf[y, c] = activated(total)
-    h_args = (hbuf, h_send, h_recv, hf_send, hf_recv)
-    gather_start(*h_args)
-
+    arrivals(1)
+    experts(1)
+    pair_add(1)
+    hub(0)
+    hub(1)
+    own(0)
+    own(1)
+    gathers[0][1]()
     def shared_on(i):
         yy = 2 * i + c
 
@@ -488,34 +585,25 @@
             rdma(shbuf.at[yy], shbuf.at[yy], shf_send.at[i], shf_recv.at[yy], partner).start()
 
     each(0, ny2, shared_on)
-    gather_pass_on(*h_args)
-
-    def expert_rows():
-        rows = hbuf[...].reshape(nslot, ffe)
-        return by_expert(rows)
-
-    loads[6].wait()
-    ret_out[...] = dot(expert_rows(), wd[...]).astype(BF16).reshape(nsp, per_dest, feat)
-
-    def give_back(i):
-        to = lax.rem(sp + i, nsp)
-        return rdma(ret_out.at[to], ret_in.at[sp], r_send.at[i], r_recv.at[sp], (to, tp))
-
-    each(1, nsp, lambda i: give_back(i).start())
-    ret_in[sp] = ret_out[sp]
+    gathers[1][1]()
+    gathers[0][2]()
+    loads[13].wait()
+    down(0)
+    gathers[1][2]()
+    down(1)
 
     def shared_arrive(i):
         yy = 2 * i + 1 - c
         rdma(shbuf.at[yy], shbuf.at[yy], shf_send.at[i], shf_recv.at[yy], partner).wait_recv()
 
     each(0, ny2, shared_arrive)
-    loads[5].wait()
+    loads[14].wait()
     base = mixed_ref[...].astype(F32) + dot(shbuf[...].reshape(tok, ffe), sd[...])
 
     each(1, nx, lambda i: kv_copy(i).wait_send())
     each(1, z + 1, lambda i: q_copy(i).wait_send())
     each(1, nz - z, lambda i: part_copy(z + i).wait_send())
-    gather_drain(*a_args)
+    a_drain()
     each(1, nsp, lambda i: dispatch(i).wait_send())
     each(0, ny2, lambda i: spre_copy(i).wait_send())
 
@@ -525,9 +613,13 @@
             srs_copy(i).wait_send()
 
     each(0, ny2, srs_drain)
-    each(0, ny, lambda i: pre_copy(i).wait_send())
-    each(0, ny - 1, lambda i: rs_copy(i).wait_send())
-    gather_drain(*h_args)
+    for g in range(2):
+        pre_copy(g).wait_send()
+        for r in (4, 3, 5, 2, 6):
+            l1_copy(g, r).wait_send()
+        for side in range(2):
+            l2_copy(g, side).wait_send()
+        gathers[g][3]()
 
     @pl.when(owner)
     def _():
@@ -544,8 +636,8 @@
     each(0, ny2, shared_forwarded)
 
     def returned(i):
-        src = lax.rem(sp + i, nsp)
-        rdma(ret_in.at[src], ret_in.at[src], r_send.at[i], r_recv.at[src], (src, tp)).wait_recv()
+        src = block_at(i, -1)
+        rdma(ret_in.at[src], ret_in.at[src], r_send.at[i], r_recv.at[i], (src, tp)).wait_recv()
 
     each(1, nsp, returned)
     rows = ret_in[...].reshape(nslot, feat)
@@ -579,7 +671,7 @@
     ffs = shared_gate.shape[1]
     cap = 2 * expert_ids.shape[1] * tok // (experts_local * nsp)
     per_dest = experts_local * cap
-    chunk = nsp * per_dest // ntp
+    chunk = nsp * per_dest // ntp // 2
     srows = tok // ny
     wide = 2 * ffe + 128
     hk = (nx // 2) * tok
@@ -588,9 +680,15 @@
         return pltpu.VMEM(shape, BF16)
 
     def sems(*counts):
-        return [pltpu.SemaphoreType.DMA((n,)) for n in counts]
+        return [pltpu.SemaphoreType.DMA(n if isinstance(n, tuple) else (n,)) for n in counts]
 
     scratch = [
+        vm(tok, hd),
+        vm(1, tok),
+        vm(tok, feat),
+        pltpu.VMEM((1, feat), F32),
+        pltpu.VMEM((2, tok), jnp.int32),
+        pltpu.VMEM((2, tok), F32),
         vm(*out_proj.shape),
         vm(experts_local * feat, ffe),
         vm(experts_local * feat, ffe),
@@ -603,35 +701,36 @@
         vm(nz, tok + 16, hd),
         vm(nz, tok + 16, hd),
         vm(hk, hk),
-        vm(ny, 2, tok, hd),
+        vm(2, ny, tok, hd),
         vm(nsp * per_dest, tok),
         vm(tok, nsp * per_dest),
         vm(tok, nsp * per_dest),
         vm(tok, feat),
         vm(nsp, per_dest, feat),
         vm(nsp, per_dest, feat),
-        vm(ntp, chunk, wide),
-        vm(ny, chunk, wide),
-        vm(ny, chunk, wide),
-        vm(ny, chunk, wide),
+        vm(2, 2, ny, chunk, wide),
+        vm(2, ny, chunk, wide),
+        vm(2, ny, chunk, wide),
+        vm(2, 2, 3, chunk, wide),
+        vm(2, 2, chunk, wide),
+        vm(2, 2, chunk, wide),
         vm(ny, srows, wide),
         vm(ny // 2, srows, wide),
         vm(ny // 2, srows, wide),
         vm(ny, srows, wide),
-        vm(ny, 2, chunk, ffe),
+        vm(2, 2, ny, chunk, ffe),
         vm(ny, srows, ffs),
         vm(nsp, per_dest, feat),
         vm(nsp, per_dest, feat),
-        *sems(7, nx, nx, nz, nz, nz, nz, ny, ny, ny, ny, nsp, nsp, ny, ny, ny, ny),
-        *sems(ny // 2, ny // 2, ny // 2, ny, ny, ny, ny, ny, ny, ny, ny // 2, ny, nsp, nsp),
+        *sems(15, nx, nx, nz, nz, nz, nz, 7, ny, ny, ny, nsp, nsp, 2, 2, (2, ny), (2, 2, 3), (2, 2), (2, 2)),
+        *sems(ny // 2, ny // 2, ny // 2, ny, (2, 7), (2, ny), (2, ny), (2, ny), ny, ny, ny // 2, ny, nsp, nsp),
     ]
-    small = pl.BlockSpec(memory_space=pltpu.VMEM)
     large = pl.BlockSpec(memory_space=pl.ANY)
     return pl.pallas_call(
         functools.partial(layer_kernel, (nz, nx, ny)),
         out_shape=jax.ShapeDtypeStruct((tok, feat), BF16),
-        in_specs=[small] * 8 + [large] * 7,
-        out_specs=small,
+        in_specs=[large] * 15,
+        out_specs=pl.BlockSpec(memory_space=pltpu.VMEM),
         scratch_shapes=scratch,
         compiler_params=pltpu.CompilerParams(
             collective_id=0, has_side_effects=True, vmem_limit_bytes=60 * 1024 * 1024
@@ -640,11 +739,11 @@
         queries,
         key_rows,
         value_rows,
-        break_bias,
+        break_bias.T,
         stream,
         norm_gain.reshape(1, feat),
-        expert_ids,
-        route_weights,
+        expert_ids.T,
+        route_weights.T,
         out_proj,
         gate_proj.reshape(experts_local * feat, ffe),
         up_proj.reshape(experts_local * feat, ffe),

time: 90.7 us -> 81.6 us (0.90)
  Pallas kernels: 86.1 us -> 79.9 us
  local copies, waits for them, and re-layouts: 4.34 us -> 1.47 us
    pallas_call x1, Pallas kernels: 86.1 us -> 79.9 us  [body(): pl.pallas_call(functools.partial(layer_kernel, (nz, nx, ny)), out_shape=j...]
    unnamed x10 -> x1, local copies, waits for them, and re-layouts: 4.34 us -> 1.47 us
where the time goes in v2:
time: 81.6 us; the launch traced here: 81.4 us
  Pallas kernels  79.9 us (98%)
  local copies, waits for them, and re-layouts  1.47 us (2%)
    pallas_call x1, Pallas kernels, body(): pl.pallas_call(functools.partial(layer_kernel, (nz, nx, ny)), out_shape=j...  79.9 us

profile of v2, /device:TPU:1, one launch (start us, length us, event | category | flops | bytes accessed | tf_op | source)
XLA Modules:
  0.0 81.4 jit_solution(4148834402910347824)
XLA Ops:
  0.0 79.9 %shard_map.145 = bf16[128,256]{1,0:T(8,128)(2,1)} custom-call(bf16[128,128]{1,0:T(8,128)(2,1)} %q_hbm.1, bf16[128,128]{1,0:T(8,128)(2,1)} %k_hbm.1, bf16[128,128]{1,0:T(8,128)(2,1)} %v_hbm.1, bf16[1,128]{1,0:T(2,128)(2,1)} %bitcast.13, bf16[128,256]{1,0:T(8,128)(2,1)} %stream_hbm.1, f32[1,256]{1,0:T(1,128)} %bitcast.10, s32[2,128]{1,0:T(2,128)} %bitcast.11, ...), custom_call_target="tpu_custom_call" | custom-call | tf_op jit(solution)/shard_map/pallas_call | solution.py:729
  79.9 1.5 %copy.17 = bf16[128,256]{1,0:T(8,128)(2,1)} copy(bf16[128,256]{1,0:T(8,128)(2,1)} %shard_map.145) | data formatting | bytes 131072

commit v3 on v2

--- a/solution.py
+++ b/solution.py
@@ -28,7 +28,7 @@
 
 
 def offset_near(i, n):
-    half = i // 2 + 1
+    half = lax.div(i, 2) + 1
     return jnp.where(lax.rem(i, 2) == 0, half, n - half)
 
 
@@ -92,8 +92,6 @@
     mixed_ref,
     snd,
     arr,
-    part,
-    pre,
     red,
     hub_in,
     hub_out,
@@ -119,8 +117,8 @@
     af_recv,
     d_send,
     d_recv,
-    pre_send,
-    pre_recv,
+    w_send,
+    w_recv,
     l1_send,
     l1_recv,
     l2_send,
@@ -131,8 +129,6 @@
     srs_recv,
     h_send,
     h_recv,
-    hf_send,
-    hf_recv,
     sh_send,
     sh_recv,
     shf_send,
@@ -144,7 +140,7 @@
     nsp, ntp = nz * nx, ny * 2
     tok, hd = q_ref.shape
     feat = stream_ref.shape[1]
-    ffe = wg.shape[1]
+    ffe = wg.shape[3]
     nslot = nsp * snd.shape[1]
     per_dest = snd.shape[1]
     cap = per_dest // 2
@@ -185,13 +181,13 @@
                 (ids_hbm, ids_ref),
                 (rw_hbm, rw_ref),
                 (stream_hbm, stream_ref),
-                (gain_hbm, gain_ref),
+                (gain_hbm, gain_ref.at[c]),
                 (wo_hbm, wo),
                 (sg_hbm, sg),
                 (su_hbm, su),
-                (wg_hbm, wg),
-                (wu_hbm, wu),
-                (wd_hbm, wd),
+                (wg_hbm, wg.at[:, c]),
+                (wu_hbm, wu.at[:, c]),
+                (wd_hbm, wd.at[c]),
                 (sd_hbm, sd),
             ]
         )
@@ -225,6 +221,14 @@
 
     each(1, nx, lambda i: kv_copy(i).start())
     each(1, z + 1, lambda i: q_copy(i).start())
+
+    swapped = [
+        rdma(mine, mine, w_send.at[i], w_recv.at[i], partner)
+        for i, mine in enumerate((wg.at[:, c], wu.at[:, c], wd.at[c], gain_ref.at[c]))
+    ]
+    for i, copy in zip((11, 12, 13, 7), swapped):
+        loads[i].wait()
+        copy.start()
 
     loads[4].wait()
     loads[5].wait()
@@ -328,9 +332,9 @@
 
     far_first = (4, 3, 5, 2, 6, 1, 7)
 
-    def gather(buf, send, recv, fsend, frecv):
+    def gather(buf, send, recv, fsend=None, frecv=None):
         def block_copy(k, block, off):
-            here = buf.at[c, block]
+            here = buf.at[c, block] if fsend is not None else buf.at[block]
             return rdma(here, here, send.at[k], recv.at[block], in_column(lax.rem(y + off, ny)))
 
         def across(block):
@@ -340,13 +344,15 @@
         def start():
             for k, off in enumerate(far_first):
                 block_copy(k, y, off).start()
-            across(y).start()
+            if fsend is not None:
+                across(y).start()
 
         def pass_on():
             for k, off in enumerate(far_first):
                 block = lax.rem(y + ny - off, ny)
                 block_copy(k, block, off).wait_recv()
-                across(block).start()
+                if fsend is not None:
+                    across(block).start()
 
         def finish():
             def arrive(block):
@@ -358,7 +364,8 @@
         def drain():
             for k, off in enumerate(far_first):
                 block_copy(k, y, off).wait_send()
-            each(0, ny, lambda block: across(block).wait_send())
+            if fsend is not None:
+                each(0, ny, lambda block: across(block).wait_send())
 
         return start, pass_on, finish, drain
 
@@ -379,22 +386,31 @@
     snd[...] = dot(pt[...], mixed).astype(BF16).reshape(nsp, per_dest, feat)
 
     def block_at(i, sign):
-        rank = i // nx
+        rank = lax.div(i, nx)
         dz = jnp.where(rank == 0, 0, offset_near(rank - 1, nz))
         dx = lax.rem(i, nx)
         return lax.rem(z + sign * dz + nz, nz) * nx + lax.rem(x + sign * dx + nx, nx)
 
     def dispatch(i):
         to = block_at(i, -1)
-        return rdma(snd.at[to], arr.at[i], d_send.at[i], d_recv.at[i], (to, tp))
+        at, core = lax.div(i, 2), lax.rem(i, 2)
+        return rdma(snd.at[to], arr.at[at, c], d_send.at[i], d_recv.at[at, c], (to, y * 2 + core))
+
+    def dispatch_own():
+        return rdma(snd.at[sp], arr.at[0, c], d_send.at[0], d_recv.at[0, c], partner)
 
     each(1, nsp, lambda i: dispatch(i).start())
-    arr[0] = snd[sp]
-
-    loads[7].wait()
-    gain = gain_ref[...]
-
-    def products(rows, lhs_of, gate_w, up_w):
+
+    @pl.when(c == 0)
+    def _():
+        arr[0, 0] = snd[sp]
+
+    @pl.when(c == 1)
+    def _():
+        dispatch_own().start()
+
+
+    def products(rows, gain, lhs_of, gate_w, up_w):
         value = rows.astype(F32)
         squares = jnp.sum(value * value, axis=1, keepdims=True)
         lhs = lhs_of((value * gain).astype(BF16))
@@ -424,7 +440,7 @@
 
     loads[9].wait()
     loads[10].wait()
-    gate, up, squares = products(mixed, lambda a: a, sg[...], su[...])
+    gate, up, squares = products(mixed, gain_ref[c], lambda a: a, sg[...], su[...])
     laid(spart, 0, gate)
     laid(spart, ffe, up)
     laid(spart, 2 * ffe, squares)
@@ -453,28 +469,41 @@
 
     each(0, ny2, shared_add)
 
-    npos, rows_g, chunk = nsp // 2, nslot // 2, part.shape[3]
+    npos, chunk = nsp // 4, red.shape[2]
+    rows_g = npos * per_dest
 
     def by_expert(a):
         zero = jnp.zeros_like(a)
         mine = lax.rem(iota(a.shape, 0), per_dest) < cap
         return jnp.concatenate([jnp.where(mine, a, zero), jnp.where(mine, zero, a)], axis=1)
 
-    def pre_copy(g):
-        return rdma(part.at[g, 1 - c], pre.at[g], pre_send.at[g], pre_recv.at[g], partner)
-
     def arrivals(g):
-        def arrive(i):
-            rdma(arr.at[i], arr.at[i], d_send.at[i], d_recv.at[i], partner).wait_recv()
+        def arrive(at):
+            for core in range(2):
+                here = arr.at[at, core]
+                rdma(here, here, d_send.at[1], d_recv.at[at, core], partner).wait_recv()
 
         each(max(1, g * npos), (g + 1) * npos, arrive)
+        if g == 0:
+            here = arr.at[0, 1]
+            rdma(here, here, d_send.at[1], d_recv.at[0, 1], partner).wait_recv()
+
+            @pl.when(c == 1)
+            def _():
+                here = arr.at[0, 0]
+                rdma(here, here, d_send.at[1], d_recv.at[0, 0], partner).wait_recv()
 
     def experts(g):
-        rows = arr[g * npos : (g + 1) * npos].reshape(rows_g, feat)
-        gate, up, squares = products(rows, by_expert, wg[...], wu[...])
+        at = slice(g * npos, (g + 1) * npos)
+        rows = jnp.concatenate([arr[at, core].reshape(rows_g, feat) for core in range(2)], axis=1)
+        gain = jnp.concatenate([gain_ref[0], gain_ref[1]], axis=1)
+        gate, up, squares = products(
+            rows, gain, by_expert, wg[...].reshape(4 * feat, ffe), wu[...].reshape(4 * feat, ffe)
+        )
         for lo, value in ((0, gate), (ffe, up), (2 * ffe, squares)):
-            part[g, :, :, :, lo : lo + value.shape[1]] = value.reshape(2, ny, chunk, value.shape[1])
-        pre_copy(g).start()
+            red[g, :, :, lo : lo + value.shape[1]] = value.reshape(ny, chunk, value.shape[1])
+        for r in (4, 3, 5, 2, 6):
+            l1_copy(g, r).start()
 
     def l1_copy(g, r):
         if r == 4:
@@ -491,15 +520,6 @@
             in_column(lax.rem(y + hub, ny)),
         )
 
-    def pair_add(g):
-        pre_copy(g).wait_recv()
-        both = part[g, c].astype(F32) + pre[g].astype(F32)
-        sums, squares = packed(both.reshape(ny * chunk, both.shape[-1]))
-        red[g, :, :, 0 : 2 * ffe] = sums.reshape(ny, chunk, 2 * ffe)
-        red[g, :, :, 2 * ffe : 2 * ffe + 128] = squares.reshape(ny, chunk, 128)
-        for r in (4, 3, 5, 2, 6):
-            l1_copy(g, r).start()
-
     def l2_copy(g, side):
         to = lax.rem(y + (1 if side == 0 else ny - 1), ny)
         return rdma(hub_out.at[g, side], own_in.at[g, side], l2_send.at[g, side], l2_recv.at[g, side], in_column(to))
@@ -519,7 +539,7 @@
             hub_out[g, side, :, 2 * ffe : 2 * ffe + 128] = squares
             l2_copy(g, side).start()
 
-    gathers = [gather(hbuf.at[g], h_send.at[g], h_recv.at[g], hf_send.at[g], hf_recv.at[g]) for g in range(2)]
+    gathers = [gather(hbuf.at[g], h_send.at[g], h_recv.at[g]) for g in range(2)]
 
     def own(g):
         total = red[g, y].astype(F32)
@@ -527,27 +547,42 @@
             here = own_in.at[g, side]
             rdma(here, here, l2_send.at[g, side], l2_recv.at[g, side], partner).wait_recv()
             total = total + own_in[g, side].astype(F32)
-        hbuf[g, c, y] = activated(total)
+        hbuf[g, y] = activated(total)
         gathers[g][0]()
 
-    def give_back(i):
+    def give_back(at, core):
+        i = 2 * at + c
         to = block_at(i, 1)
-        return rdma(ret_out.at[i], ret_in.at[sp], r_send.at[i], r_recv.at[i], (to, tp))
+        return rdma(ret_out.at[at, core], ret_in.at[sp], r_send.at[at, core], r_recv.at[i], (to, y * 2 + core))
 
     def down(g):
         rows = by_expert(hbuf[g].reshape(rows_g, ffe))
-        ret_out[g * npos : (g + 1) * npos] = dot(rows, wd[...]).astype(BF16).reshape(npos, per_dest, feat)
-        each(max(1, g * npos), (g + 1) * npos, lambda i: give_back(i).start())
+        at = slice(g * npos, (g + 1) * npos)
+        for core in range(2):
+            ret_out[at, core] = dot(rows, wd[core]).astype(BF16).reshape(npos, per_dest, feat)
+
+        def back(at):
+            for core in range(2):
+                give_back(at, core).start()
+
+        each(max(1, g * npos), (g + 1) * npos, back)
         if g == 0:
-            ret_in[sp] = ret_out[0]
+            give_back(0, 1).start()
+
+            @pl.when(c == 1)
+            def _():
+                give_back(0, 0).start()
+
+            @pl.when(c == 0)
+            def _():
+                ret_in[sp] = ret_out[0, 0]
 
     owner = lax.rem(y, 2) == c
 
     arrivals(0)
-    loads[11].wait()
-    loads[12].wait()
+    for i in (0, 1, 3):
+        swapped[i].wait_recv()
     experts(0)
-    pair_add(0)
 
     @pl.when(owner)
     def _():
@@ -570,7 +605,6 @@
 
     arrivals(1)
     experts(1)
-    pair_add(1)
     hub(0)
     hub(1)
     own(0)
@@ -585,11 +619,9 @@
             rdma(shbuf.at[yy], shbuf.at[yy], shf_send.at[i], shf_recv.at[yy], partner).start()
 
     each(0, ny2, shared_on)
+    swapped[2].wait_recv()
+    down(0)
     gathers[1][1]()
-    gathers[0][2]()
-    loads[13].wait()
-    down(0)
-    gathers[1][2]()
     down(1)
 
     def shared_arrive(i):
@@ -605,6 +637,13 @@
     each(1, nz - z, lambda i: part_copy(z + i).wait_send())
     a_drain()
     each(1, nsp, lambda i: dispatch(i).wait_send())
+
+    @pl.when(c == 1)
+    def _():
+        dispatch_own().wait_send()
+
+    for copy in swapped:
+        copy.wait_send()
     each(0, ny2, lambda i: spre_copy(i).wait_send())
 
     def srs_drain(i):
@@ -614,7 +653,6 @@
 
     each(0, ny2, srs_drain)
     for g in range(2):
-        pre_copy(g).wait_send()
         for r in (4, 3, 5, 2, 6):
             l1_copy(g, r).wait_send()
         for side in range(2):
@@ -640,9 +678,24 @@
         rdma(ret_in.at[src], ret_in.at[src], r_send.at[i], r_recv.at[i], (src, tp)).wait_recv()
 
     each(1, nsp, returned)
+
+    @pl.when(c == 1)
+    def _():
+        returned(0)
+
     rows = ret_in[...].reshape(nslot, feat)
     out_ref[...] = (base + (dot(w_hi[...], rows) + dot(w_lo[...], rows))).astype(BF16)
-    each(1, nsp, lambda i: give_back(i).wait_send())
+
+    def given(at):
+        for core in range(2):
+            give_back(at, core).wait_send()
+
+    each(1, nsp // 2, given)
+    give_back(0, 1).wait_send()
+
+    @pl.when(c == 1)
+    def _():
+        give_back(0, 0).wait_send()
 
 
 def body(
@@ -686,13 +739,13 @@
         vm(tok, hd),
         vm(1, tok),
         vm(tok, feat),
-        pltpu.VMEM((1, feat), F32),
+        pltpu.VMEM((2, 1, feat), F32),
         pltpu.VMEM((2, tok), jnp.int32),
         pltpu.VMEM((2, tok), F32),
         vm(*out_proj.shape),
-        vm(experts_local * feat, ffe),
-        vm(experts_local * feat, ffe),
-        vm(experts_local * ffe, feat),
+        vm(experts_local, 2, feat, ffe),
+        vm(experts_local, 2, feat, ffe),
+        vm(2, experts_local * ffe, feat),
         vm(feat, ffs),
         vm(feat, ffs),
         vm(ffs, feat),
@@ -707,9 +760,7 @@
         vm(tok, nsp * per_dest),
         vm(tok, feat),
         vm(nsp, per_dest, feat),
-        vm(nsp, per_dest, feat),
-        vm(2, 2, ny, chunk, wide),
-        vm(2, ny, chunk, wide),
+        vm(nsp // 2, 2, per_dest, feat),
         vm(2, ny, chunk, wide),
         vm(2, 2, 3, chunk, wide),
         vm(2, 2, chunk, wide),
@@ -718,12 +769,12 @@
         vm(ny // 2, srows, wide),
         vm(ny // 2, srows, wide),
         vm(ny, srows, wide),
-        vm(2, 2, ny, chunk, ffe),
+        vm(2, ny, chunk, ffe),
         vm(ny, srows, ffs),
+        vm(nsp // 2, 2, per_dest, feat),
         vm(nsp, per_dest, feat),
-        vm(nsp, per_dest, feat),
-        *sems(15, nx, nx, nz, nz, nz, nz, 7, ny, ny, ny, nsp, nsp, 2, 2, (2, ny), (2, 2, 3), (2, 2), (2, 2)),
-        *sems(ny // 2, ny // 2, ny // 2, ny, (2, 7), (2, ny), (2, ny), (2, ny), ny, ny, ny // 2, ny, nsp, nsp),
+        *sems(15, nx, nx, nz, nz, nz, nz, 7, ny, ny, ny, nsp, (nsp // 2, 2), 4, 4, (2, ny), (2, 2, 3), (2, 2), (2, 2)),
+        *sems(ny // 2, ny // 2, ny // 2, ny, (2, 7), (2, ny), ny, ny, ny // 2, ny, (nsp // 2, 2), nsp),
     ]
     large = pl.BlockSpec(memory_space=pl.ANY)
     return pl.pallas_call(
@@ -745,8 +796,8 @@
         expert_ids.T,
         route_weights.T,
         out_proj,
-        gate_proj.reshape(experts_local * feat, ffe),
-        up_proj.reshape(experts_local * feat, ffe),
+        gate_proj,
+        up_proj,
         down_proj.reshape(experts_local * ffe, feat),
         shared_gate,
         shared_up,

time: 81.6 us -> 79.3 us (0.972)
  Pallas kernels: 79.9 us -> 77.6 us
    pallas_call x1, Pallas kernels: 79.9 us -> 77.6 us  [body(): pl.pallas_call(functools.partial(layer_kernel, (nz, nx, ny)), out_shape=j...]
where the time goes in v3:
time: 79.3 us; the launch traced here: 79.1 us
  Pallas kernels  77.6 us (98%)
  local copies, waits for them, and re-layouts  1.47 us (2%)
    pallas_call x1, Pallas kernels, body(): pl.pallas_call(functools.partial(layer_kernel, (nz, nx, ny)), out_shape=j...  77.6 us

profile of v3, /device:TPU:1, one launch (start us, length us, event | category | flops | bytes accessed | tf_op | source)
XLA Modules:
  0.0 79.1 jit_solution(14179674313927978836)
XLA Ops:
  0.0 77.6 %shard_map.145 = bf16[128,256]{1,0:T(8,128)(2,1)} custom-call(bf16[128,128]{1,0:T(8,128)(2,1)} %q_hbm.1, bf16[128,128]{1,0:T(8,128)(2,1)} %k_hbm.1, bf16[128,128]{1,0:T(8,128)(2,1)} %v_hbm.1, bf16[1,128]{1,0:T(2,128)(2,1)} %bitcast.9, bf16[128,256]{1,0:T(8,128)(2,1)} %stream_hbm.1, f32[1,256]{1,0:T(1,128)} %bitcast.6, s32[2,128]{1,0:T(2,128)} %bitcast.7, ...), custom_call_target="tpu_custom_call" | custom-call | tf_op jit(solution)/shard_map/pallas_call | solution.py:780
  77.6 1.5 %copy.17 = bf16[128,256]{1,0:T(8,128)(2,1)} copy(bf16[128,256]{1,0:T(8,128)(2,1)} %shard_map.145) | data formatting | bytes 131072

commit v4 on v3

--- a/solution.py
+++ b/solution.py
@@ -159,16 +159,19 @@
 
     barrier = pltpu.get_barrier_semaphore()
 
-    def greet_sp(i):
-        pl.semaphore_signal(
-            barrier, inc=1, device_id=(lax.rem(sp + i, nsp), tp), device_id_type=MESH
-        )
+    def greet_row(i):
+        to = z * nx + lax.rem(x + i, nx)
+        pl.semaphore_signal(barrier, inc=1, device_id=(to, tp), device_id_type=MESH)
+
+    def greet_later(zz):
+        pl.semaphore_signal(barrier, inc=1, device_id=(zz * nx + x, tp), device_id_type=MESH)
 
     def greet_tp(i):
         pl.semaphore_signal(barrier, inc=1, device_id=in_column(lax.rem(y + i, ny)), device_id_type=MESH)
 
-    each(1, nsp, greet_sp)
     each(1, ny, greet_tp)
+    each(z + 1, nz, greet_later)
+    each(1, nx, greet_row)
     pl.semaphore_signal(barrier, inc=1, device_id=partner, device_id_type=MESH)
     loads = [
         load(i, src, dst)
@@ -210,7 +213,7 @@
     for i in (1, 2, 3):
         loads[i].wait()
 
-    pl.semaphore_wait(barrier, nsp - 1 + ny)
+    pl.semaphore_wait(barrier, nx - 1 + ny + z)
 
     def kv_copy(i):
         peer = lax.rem(x + i, nx)
@@ -293,13 +296,6 @@
     def part_copy(zq):
         return rdma(part_out.at[zq], part_in.at[z], p_send.at[zq], p_recv.at[z], (zq * nx + x, tp))
 
-    def serve_far_first(i):
-        off = offset_near(nz - 2 - i, nz)
-
-        @pl.when(z + off < nz)
-        def _():
-            serve(off)
-
     def serve(i):
         zq = z + i
         rdma(qbuf.at[zq], qbuf.at[zq], q_send.at[i], q_recv.at[zq], (zq * nx + x, tp)).wait_recv()
@@ -317,7 +313,7 @@
         part_out[zq, tok : tok + 16, :] = rows.astype(BF16)
         part_copy(zq).start()
 
-    each(0, nz - 1, serve_far_first)
+    each(1, nz - z, serve)
     acc, later = attend(q_ref[...], True)
 
     def combine(i, carry):

time: 79.3 us -> 76.1 us (0.960)
  Pallas kernels: 77.6 us -> 74.4 us
    pallas_call x1, Pallas kernels: 77.6 us -> 74.4 us  [body(): pl.pallas_call(functools.partial(layer_kernel, (nz, nx, ny)), out_shape=j...]
where the time goes in v4:
time: 76.1 us; the launch traced here: 75.9 us
  Pallas kernels  74.4 us (98%)
  local copies, waits for them, and re-layouts  1.47 us (2%)
    pallas_call x1, Pallas kernels, body(): pl.pallas_call(functools.partial(layer_kernel, (nz, nx, ny)), out_shape=j...  74.4 us

profile of v4, /device:TPU:1, one launch (start us, length us, event | category | flops | bytes accessed | tf_op | source)
XLA Modules:
  0.0 75.9 jit_solution(9176525685244501941)
XLA Ops:
  0.0 74.4 %shard_map.145 = bf16[128,256]{1,0:T(8,128)(2,1)} custom-call(bf16[128,128]{1,0:T(8,128)(2,1)} %q_hbm.1, bf16[128,128]{1,0:T(8,128)(2,1)} %k_hbm.1, bf16[128,128]{1,0:T(8,128)(2,1)} %v_hbm.1, bf16[1,128]{1,0:T(2,128)(2,1)} %bitcast.9, bf16[128,256]{1,0:T(8,128)(2,1)} %stream_hbm.1, f32[1,256]{1,0:T(1,128)} %bitcast.6, s32[2,128]{1,0:T(2,128)} %bitcast.7, ...), custom_call_target="tpu_custom_call" | custom-call | tf_op jit(solution)/shard_map/pallas_call | solution.py:776
  74.4 1.5 %copy.17 = bf16[128,256]{1,0:T(8,128)(2,1)} copy(bf16[128,256]{1,0:T(8,128)(2,1)} %shard_map.145) | data formatting | bytes 131072

commit v5 on v4

--- a/solution.py
+++ b/solution.py
@@ -96,6 +96,8 @@
     hub_in,
     hub_out,
     own_in,
+    square_rows,
+    inverse,
     spart,
     spre,
     sred,
@@ -123,6 +125,8 @@
     l1_recv,
     l2_send,
     l2_recv,
+    n_send,
+    n_recv,
     spre_send,
     spre_recv,
     srs_send,
@@ -185,13 +189,14 @@
                 (rw_hbm, rw_ref),
                 (stream_hbm, stream_ref),
                 (gain_hbm, gain_ref.at[c]),
-                (wo_hbm, wo),
+                (wo_hbm.at[:, 0], wo.at[0]),
                 (sg_hbm, sg),
                 (su_hbm, su),
                 (wg_hbm, wg.at[:, c]),
                 (wu_hbm, wu.at[:, c]),
                 (wd_hbm, wd.at[c]),
                 (sd_hbm, sd),
+                (wo_hbm.at[:, 1], wo.at[1]),
             ]
         )
     ]
@@ -369,23 +374,36 @@
     a_start, a_pass, a_finish, a_drain = gather(abuf, a_send, a_recv, af_send, af_recv)
     a_start()
     a_pass()
+    loads[8].wait()
+    loads[15].wait()
+    loads[6].wait()
+
+    def project(core):
+        total = jnp.zeros((tok, feat), F32)
+        for i in range(0, ny, 2):
+            heads = jnp.concatenate([abuf[core, i], abuf[core, i + 1]], axis=1)
+            total = total + dot(heads, wo[core, i : i + 2].reshape(2 * hd, feat))
+        return total
+
+    projected = stream_ref[...].astype(F32) + project(c)
     a_finish()
-    loads[8].wait()
-    loads[6].wait()
-    projected = jnp.zeros((tok, feat), F32)
-    for i in range(ny):
-        heads = jnp.concatenate([abuf[0, i], abuf[1, i]], axis=1)
-        projected = projected + dot(heads, wo[i * 2 * hd : (i + 1) * 2 * hd, :])
-    mixed = (stream_ref[...].astype(F32) + projected).astype(BF16)
+    projected = projected + project(1 - c)
+    mixed = projected.astype(BF16)
     mixed_ref[...] = mixed
 
     snd[...] = dot(pt[...], mixed).astype(BF16).reshape(nsp, per_dest, feat)
 
     def block_at(i, sign):
         rank = lax.div(i, nx)
-        dz = jnp.where(rank == 0, 0, offset_near(rank - 1, nz))
+        dz = jnp.where(rank == nz - 1, 0, offset_near(nz - 2 - rank, nz))
         dx = lax.rem(i, nx)
         return lax.rem(z + sign * dz + nz, nz) * nx + lax.rem(x + sign * dx + nx, nx)
+
+    own_i, own_at = (nz - 1) * nx, (nz - 1) * nx // 2
+
+    def others(fn):
+        each(0, own_i, fn)
+        each(own_i + 1, nsp, fn)
 
     def dispatch(i):
         to = block_at(i, -1)
@@ -393,13 +411,13 @@
         return rdma(snd.at[to], arr.at[at, c], d_send.at[i], d_recv.at[at, c], (to, y * 2 + core))
 
     def dispatch_own():
-        return rdma(snd.at[sp], arr.at[0, c], d_send.at[0], d_recv.at[0, c], partner)
-
-    each(1, nsp, lambda i: dispatch(i).start())
+        return rdma(snd.at[sp], arr.at[own_at, c], d_send.at[own_i], d_recv.at[own_at, c], partner)
+
+    others(lambda i: dispatch(i).start())
 
     @pl.when(c == 0)
     def _():
-        arr[0, 0] = snd[sp]
+        arr[own_at, 0] = snd[sp]
 
     @pl.when(c == 1)
     def _():
@@ -412,7 +430,7 @@
         lhs = lhs_of((value * gain).astype(BF16))
         gate = dot(lhs, gate_w).astype(BF16)
         up = dot(lhs, up_w).astype(BF16)
-        return gate, up, two_lanes(squares)
+        return gate, up, squares
 
     def two_lanes(column):
         high, low = halves(column)
@@ -430,7 +448,9 @@
 
     def activated(total):
         squares = total[:, 2 * ffe : 2 * ffe + 1] + total[:, 2 * ffe + 1 : 2 * ffe + 2]
-        inv = lax.rsqrt(squares / width + EPS)
+        return scaled_hidden(total, lax.rsqrt(squares / width + EPS))
+
+    def scaled_hidden(total, inv):
         gate, up = total[:, 0:ffe] * inv, total[:, ffe : 2 * ffe] * inv
         return (gate * jax.nn.sigmoid(gate) * up).astype(BF16)
 
@@ -439,7 +459,7 @@
     gate, up, squares = products(mixed, gain_ref[c], lambda a: a, sg[...], su[...])
     laid(spart, 0, gate)
     laid(spart, ffe, up)
-    laid(spart, 2 * ffe, squares)
+    laid(spart, 2 * ffe, two_lanes(squares))
     ny2 = ny // 2
 
     def spre_copy(i):
@@ -479,15 +499,35 @@
                 here = arr.at[at, core]
                 rdma(here, here, d_send.at[1], d_recv.at[at, core], partner).wait_recv()
 
-        each(max(1, g * npos), (g + 1) * npos, arrive)
         if g == 0:
-            here = arr.at[0, 1]
-            rdma(here, here, d_send.at[1], d_recv.at[0, 1], partner).wait_recv()
+            each(0, npos, arrive)
+        else:
+            each(npos, own_at, arrive)
+            each(own_at + 1, 2 * npos, arrive)
+            here = arr.at[own_at, 1]
+            rdma(here, here, d_send.at[1], d_recv.at[own_at, 1], partner).wait_recv()
 
             @pl.when(c == 1)
             def _():
-                here = arr.at[0, 0]
-                rdma(here, here, d_send.at[1], d_recv.at[0, 0], partner).wait_recv()
+                here = arr.at[own_at, 0]
+                rdma(here, here, d_send.at[1], d_recv.at[own_at, 0], partner).wait_recv()
+
+    def squares_copy(g, k):
+        here = square_rows.at[g, y]
+        return rdma(here, here, n_send.at[g, k], n_recv.at[g, y], in_column(lax.rem(y + k, ny)))
+
+    def scales(g):
+        def arrive(k):
+            ys = lax.rem(y + k, ny)
+            here = square_rows.at[g, ys]
+            rdma(here, here, n_send.at[g, k], n_recv.at[g, ys], partner).wait_recv()
+
+        each(1, ny, arrive)
+        squares = square_rows[g, 0]
+        for ys in range(1, ny):
+            squares = squares + square_rows[g, ys]
+        inv = to_column(lax.rsqrt(squares / width + EPS))
+        inverse[g] = jnp.broadcast_to(inv, (rows_g, 128)).reshape(ny, chunk, 128)
 
     def experts(g):
         at = slice(g * npos, (g + 1) * npos)
@@ -496,8 +536,11 @@
         gate, up, squares = products(
             rows, gain, by_expert, wg[...].reshape(4 * feat, ffe), wu[...].reshape(4 * feat, ffe)
         )
-        for lo, value in ((0, gate), (ffe, up), (2 * ffe, squares)):
-            red[g, :, :, lo : lo + value.shape[1]] = value.reshape(ny, chunk, value.shape[1])
+        square_rows[g, y] = to_row(squares)
+        for k in range(1, ny):
+            squares_copy(g, k).start()
+        red[g, :, :, 0:ffe] = gate.reshape(ny, chunk, ffe)
+        red[g, :, :, ffe : 2 * ffe] = up.reshape(ny, chunk, ffe)
         for r in (4, 3, 5, 2, 6):
             l1_copy(g, r).start()
 
@@ -530,9 +573,7 @@
             odd = lax.rem(y, 2)
             mine = red[g, lax.rem(y + (1 if side == 0 else ny - 1), ny)].astype(F32)
             total = lax.fori_loop(0, 2 + odd if side == 0 else 3 - odd, add_in, mine)
-            sums, squares = packed(total)
-            hub_out[g, side, :, 0 : 2 * ffe] = sums
-            hub_out[g, side, :, 2 * ffe : 2 * ffe + 128] = squares
+            hub_out[g, side] = total.astype(BF16)
             l2_copy(g, side).start()
 
     gathers = [gather(hbuf.at[g], h_send.at[g], h_recv.at[g]) for g in range(2)]
@@ -543,7 +584,7 @@
             here = own_in.at[g, side]
             rdma(here, here, l2_send.at[g, side], l2_recv.at[g, side], partner).wait_recv()
             total = total + own_in[g, side].astype(F32)
-        hbuf[g, y] = activated(total)
+        hbuf[g, y] = scaled_hidden(total, inverse[g, y][:, 0:1])
         gathers[g][0]()
 
     def give_back(at, core):
@@ -561,17 +602,20 @@
             for core in range(2):
                 give_back(at, core).start()
 
-        each(max(1, g * npos), (g + 1) * npos, back)
         if g == 0:
-            give_back(0, 1).start()
+            each(0, npos, back)
+        else:
+            each(npos, own_at, back)
+            each(own_at + 1, 2 * npos, back)
+            give_back(own_at, 1).start()
 
             @pl.when(c == 1)
             def _():
-                give_back(0, 0).start()
+                give_back(own_at, 0).start()
 
             @pl.when(c == 0)
             def _():
-                ret_in[sp] = ret_out[0, 0]
+                ret_in[sp] = ret_out[own_at, 0]
 
     owner = lax.rem(y, 2) == c
 
@@ -602,6 +646,8 @@
     arrivals(1)
     experts(1)
     hub(0)
+    scales(0)
+    scales(1)
     hub(1)
     own(0)
     own(1)
@@ -632,7 +678,7 @@
     each(1, z + 1, lambda i: q_copy(i).wait_send())
     each(1, nz - z, lambda i: part_copy(z + i).wait_send())
     a_drain()
-    each(1, nsp, lambda i: dispatch(i).wait_send())
+    others(lambda i: dispatch(i).wait_send())
 
     @pl.when(c == 1)
     def _():
@@ -653,6 +699,8 @@
             l1_copy(g, r).wait_send()
         for side in range(2):
             l2_copy(g, side).wait_send()
+        for k in range(1, ny):
+            squares_copy(g, k).wait_send()
         gathers[g][3]()
 
     @pl.when(owner)
@@ -673,11 +721,11 @@
         src = block_at(i, -1)
         rdma(ret_in.at[src], ret_in.at[src], r_send.at[i], r_recv.at[i], (src, tp)).wait_recv()
 
-    each(1, nsp, returned)
+    others(returned)
 
     @pl.when(c == 1)
     def _():
-        returned(0)
+        returned(own_i)
 
     rows = ret_in[...].reshape(nslot, feat)
     out_ref[...] = (base + (dot(w_hi[...], rows) + dot(w_lo[...], rows))).astype(BF16)
@@ -686,12 +734,13 @@
         for core in range(2):
             give_back(at, core).wait_send()
 
-    each(1, nsp // 2, given)
-    give_back(0, 1).wait_send()
+    each(0, own_at, given)
+    each(own_at + 1, nsp // 2, given)
+    give_back(own_at, 1).wait_send()
 
     @pl.when(c == 1)
     def _():
-        give_back(0, 0).wait_send()
+        give_back(own_at, 0).wait_send()
 
 
 def body(
@@ -738,7 +787,7 @@
         pltpu.VMEM((2, 1, feat), F32),
         pltpu.VMEM((2, tok), jnp.int32),
         pltpu.VMEM((2, tok), F32),
-        vm(*out_proj.shape),
+        vm(2, ny, hd, feat),
         vm(experts_local, 2, feat, ffe),
         vm(experts_local, 2, feat, ffe),
         vm(2, experts_local * ffe, feat),
@@ -757,10 +806,12 @@
         vm(tok, feat),
         vm(nsp, per_dest, feat),
         vm(nsp // 2, 2, per_dest, feat),
-        vm(2, ny, chunk, wide),
-        vm(2, 2, 3, chunk, wide),
-        vm(2, 2, chunk, wide),
-        vm(2, 2, chunk, wide),
+        vm(2, ny, chunk, 2 * ffe),
+        vm(2, 2, 3, chunk, 2 * ffe),
+        vm(2, 2, chunk, 2 * ffe),
+        vm(2, 2, chunk, 2 * ffe),
+        pltpu.VMEM((2, ny, 1, ny * chunk), F32),
+        pltpu.VMEM((2, ny, chunk, 128), F32),
         vm(ny, srows, wide),
         vm(ny // 2, srows, wide),
         vm(ny // 2, srows, wide),
@@ -769,7 +820,7 @@
         vm(ny, srows, ffs),
         vm(nsp // 2, 2, per_dest, feat),
         vm(nsp, per_dest, feat),
-        *sems(15, nx, nx, nz, nz, nz, nz, 7, ny, ny, ny, nsp, (nsp // 2, 2), 4, 4, (2, ny), (2, 2, 3), (2, 2), (2, 2)),
+        *sems(16, nx, nx, nz, nz, nz, nz, 7, ny, ny, ny, nsp, (nsp // 2, 2), 4, 4, (2, ny), (2, 2, 3), (2, 2), (2, 2), (2, ny), (2, ny)),
         *sems(ny // 2, ny // 2, ny // 2, ny, (2, 7), (2, ny), ny, ny, ny // 2, ny, (nsp // 2, 2), nsp),
     ]
     large = pl.BlockSpec(memory_space=pl.ANY)
@@ -791,7 +842,7 @@
         norm_gain.reshape(1, feat),
         expert_ids.T,
         route_weights.T,
-        out_proj,
+        out_proj.reshape(ny, 2, hd, feat),
         gate_proj,
         up_proj,
         down_proj.reshape(experts_local * ffe, feat),

time: 76.1 us -> 74.1 us (0.974)
  Pallas kernels: 74.4 us -> 72.5 us
    pallas_call x1, Pallas kernels: 74.4 us -> 72.5 us  [body(): pl.pallas_call(functools.partial(layer_kernel, (nz, nx, ny)), out_shape=j...]
where the time goes in v5:
time: 74.1 us; the launch traced here: 74 us
  Pallas kernels  72.5 us (98%)
  local copies, waits for them, and re-layouts  1.47 us (2%)
    pallas_call x1, Pallas kernels, body(): pl.pallas_call(functools.partial(layer_kernel, (nz, nx, ny)), out_shape=j...  72.5 us

profile of v5, /device:TPU:1, one launch (start us, length us, event | category | flops | bytes accessed | tf_op | source)
XLA Modules:
  0.0 74.0 jit_solution(13686115085553020852)
XLA Ops:
  0.0 72.5 %shard_map.145 = bf16[128,256]{1,0:T(8,128)(2,1)} custom-call(bf16[128,128]{1,0:T(8,128)(2,1)} %q_hbm.1, bf16[128,128]{1,0:T(8,128)(2,1)} %k_hbm.1, bf16[128,128]{1,0:T(8,128)(2,1)} %v_hbm.1, bf16[1,128]{1,0:T(2,128)(2,1)} %bitcast.11, bf16[128,256]{1,0:T(8,128)(2,1)} %stream_hbm.1, f32[1,256]{1,0:T(1,128)} %bitcast.8, s32[2,128]{1,0:T(2,128)} %bitcast.9, ...), custom_call_target="tpu_custom_call" | custom-call | tf_op jit(solution)/shard_map/pallas_call | solution.py:827
  72.5 1.5 %copy.17 = bf16[128,256]{1,0:T(8,128)(2,1)} copy(bf16[128,256]{1,0:T(8,128)(2,1)} %shard_map.145) | data formatting | bytes 131072

commit v6 on v5

--- a/solution.py
+++ b/solution.py
@@ -218,6 +218,11 @@
     for i in (1, 2, 3):
         loads[i].wait()
 
+    def no_part(zs):
+        part_in[zs] = jnp.zeros((tok + 16, hd), BF16)
+
+    each(z + 1, nz, no_part)
+
     pl.semaphore_wait(barrier, nx - 1 + ny + z)
 
     def kv_copy(i):
@@ -319,17 +324,18 @@
         part_copy(zq).start()
 
     each(1, nz - z, serve)
-    acc, later = attend(q_ref[...], True)
-
-    def combine(i, carry):
-        acc, later = carry
+    acc, total = attend(q_ref[...], True)
+
+    def part_arrive(i):
         zs = z - i
         rdma(part_in.at[zs], part_in.at[zs], p_send.at[zs], p_recv.at[zs], (zs * nx + x, tp)).wait_recv()
-        summary = part_in[zs, 0:tok, :].astype(F32)
-        row = jnp.sum(part_in[zs, tok : tok + 16, :].astype(F32), axis=0, keepdims=True)
-        return acc + jnp.exp(later) * summary, later + to_column(row)
-
-    acc, later = lax.fori_loop(1, z + 1, combine, (acc, later))
+
+    each(1, z + 1, part_arrive)
+    later = to_row(total)
+    for i in range(1, nz):
+        zs = lax.rem(z - i + nz, nz)
+        acc = acc + to_column(jnp.exp(later)) * part_in[zs, 0:tok, :].astype(F32)
+        later = later + jnp.sum(part_in[zs, tok : tok + 16, :].astype(F32), axis=0, keepdims=True)
 
     far_first = (4, 3, 5, 2, 6, 1, 7)
 
@@ -399,7 +405,26 @@
         dx = lax.rem(i, nx)
         return lax.rem(z + sign * dz + nz, nz) * nx + lax.rem(x + sign * dx + nx, nx)
 
-    own_i, own_at = (nz - 1) * nx, (nz - 1) * nx // 2
+    half = nsp // 2
+    own_i = (nz - 1) * nx
+    own_at = own_i % half
+
+    def wrapped(value, n):
+        return jnp.where(value >= n, value - n, value)
+
+    def step_z(rank):
+        i = nz - 2 - rank
+        return 0 if rank == nz - 1 else (i // 2 + 1 if i % 2 == 0 else nz - (i // 2 + 1))
+
+    before = [wrapped(z + (nz - step_z(rank)) % nz, nz) * nx for rank in range(nz)]
+    after = [wrapped(z + step_z(rank), nz) * nx for rank in range(nz)]
+    left = [wrapped(x + (nx - dx) % nx, nx) for dx in range(nx)]
+    right = [wrapped(x + dx, nx) for dx in range(nx)]
+
+    def send_out(i):
+        to = before[i // nx] + left[i % nx]
+        at, core = i % half, 1 - i // half
+        rdma(snd.at[to], arr.at[at, c], d_send.at[i], d_recv.at[at, c], (to, y * 2 + core)).start()
 
     def others(fn):
         each(0, own_i, fn)
@@ -407,13 +432,16 @@
 
     def dispatch(i):
         to = block_at(i, -1)
-        at, core = lax.div(i, 2), lax.rem(i, 2)
+        core = jnp.where(i < half, 1, 0)
+        at = jnp.where(i < half, i, i - half)
         return rdma(snd.at[to], arr.at[at, c], d_send.at[i], d_recv.at[at, c], (to, y * 2 + core))
 
     def dispatch_own():
         return rdma(snd.at[sp], arr.at[own_at, c], d_send.at[own_i], d_recv.at[own_at, c], partner)
 
-    others(lambda i: dispatch(i).start())
+    for i in range(nsp):
+        if i != own_i:
+            send_out(i)
 
     @pl.when(c == 0)
     def _():
@@ -499,11 +527,11 @@
                 here = arr.at[at, core]
                 rdma(here, here, d_send.at[1], d_recv.at[at, core], partner).wait_recv()
 
-        if g == 0:
-            each(0, npos, arrive)
+        if g != own_at // npos:
+            each(g * npos, (g + 1) * npos, arrive)
         else:
-            each(npos, own_at, arrive)
-            each(own_at + 1, 2 * npos, arrive)
+            each(g * npos, own_at, arrive)
+            each(own_at + 1, (g + 1) * npos, arrive)
             here = arr.at[own_at, 1]
             rdma(here, here, d_send.at[1], d_recv.at[own_at, 1], partner).wait_recv()
 
@@ -588,7 +616,7 @@
         gathers[g][0]()
 
     def give_back(at, core):
-        i = 2 * at + c
+        i = at + half * (1 - c)
         to = block_at(i, 1)
         return rdma(ret_out.at[at, core], ret_in.at[sp], r_send.at[at, core], r_recv.at[i], (to, y * 2 + core))
 
@@ -598,15 +626,19 @@
         for core in range(2):
             ret_out[at, core] = dot(rows, wd[core]).astype(BF16).reshape(npos, per_dest, feat)
 
-        def back(at):
-            for core in range(2):
-                give_back(at, core).start()
-
-        if g == 0:
-            each(0, npos, back)
-        else:
-            each(npos, own_at, back)
-            each(own_at + 1, 2 * npos, back)
+        for at in range(g * npos, (g + 1) * npos):
+            if at != own_at:
+                near = at + half
+                to = jnp.where(c == 1, after[at // nx] + right[at % nx], after[near // nx] + right[near % nx])
+                for core in range(2):
+                    rdma(
+                        ret_out.at[at, core],
+                        ret_in.at[sp],
+                        r_send.at[at, core],
+                        r_recv.at[at + half * (1 - c)],
+                        (to, y * 2 + core),
+                    ).start()
+        if g == own_at // npos:
             give_back(own_at, 1).start()
 
             @pl.when(c == 1)

time: 74.1 us -> 73.1 us (0.987)
  Pallas kernels: 72.5 us -> 71.4 us
    pallas_call x1, Pallas kernels: 72.5 us -> 71.4 us  [body(): pl.pallas_call(functools.partial(layer_kernel, (nz, nx, ny)), out_shape=j...]
where the time goes in v6:
time: 73.1 us; the launch traced here: 72.9 us
  Pallas kernels  71.4 us (98%)
  local copies, waits for them, and re-layouts  1.47 us (2%)
    pallas_call x1, Pallas kernels, body(): pl.pallas_call(functools.partial(layer_kernel, (nz, nx, ny)), out_shape=j...  71.4 us
    unnamed x1, local copies, waits for them, and re-layouts  1.47 us

profile of v6, /device:TPU:1, one launch (start us, length us, event | category | flops | bytes accessed | tf_op | source)
XLA Modules:
  0.0 72.9 jit_solution(9585361537387067464)
XLA Ops:
  0.0 71.4 %shard_map.145 = bf16[128,256]{1,0:T(8,128)(2,1)} custom-call(bf16[128,128]{1,0:T(8,128)(2,1)} %q_hbm.1, bf16[128,128]{1,0:T(8,128)(2,1)} %k_hbm.1, bf16[128,128]{1,0:T(8,128)(2,1)} %v_hbm.1, bf16[1,128]{1,0:T(2,128)(2,1)} %bitcast.11, bf16[128,256]{1,0:T(8,128)(2,1)} %stream_hbm.1, f32[1,256]{1,0:T(1,128)} %bitcast.8, s32[2,128]{1,0:T(2,128)} %bitcast.9, ...), custom_call_target="tpu_custom_call" | custom-call | tf_op jit(solution)/shard_map/pallas_call | solution.py:859
  71.4 1.5 %copy.17 = bf16[128,256]{1,0:T(8,128)(2,1)} copy(bf16[128,256]{1,0:T(8,128)(2,1)} %shard_map.145) | data formatting | bytes 131072

commit v7 on v6

--- a/solution.py
+++ b/solution.py
@@ -439,7 +439,8 @@
     def dispatch_own():
         return rdma(snd.at[sp], arr.at[own_at, c], d_send.at[own_i], d_recv.at[own_at, c], partner)
 
-    for i in range(nsp):
+    for k in range(nsp):
+        i = k // 2 + half * (k % 2)
         if i != own_i:
             send_out(i)
 

time: 73.1 us -> 73 us (level)
  no operation moved by 1% of the time
where the time goes in v7:
time: 73 us; the launch traced here: 72.8 us
  Pallas kernels  71.3 us (98%)
  local copies, waits for them, and re-layouts  1.47 us (2%)
    pallas_call x1, Pallas kernels, body(): pl.pallas_call(functools.partial(layer_kernel, (nz, nx, ny)), out_shape=j...  71.3 us
    unnamed x1, local copies, waits for them, and re-layouts  1.47 us

profile of v7, /device:TPU:1, one launch (start us, length us, event | category | flops | bytes accessed | tf_op | source)
XLA Modules:
  0.0 72.8 jit_solution(18078907534183644784)
XLA Ops:
  0.0 71.3 %shard_map.145 = bf16[128,256]{1,0:T(8,128)(2,1)} custom-call(bf16[128,128]{1,0:T(8,128)(2,1)} %q_hbm.1, bf16[128,128]{1,0:T(8,128)(2,1)} %k_hbm.1, bf16[128,128]{1,0:T(8,128)(2,1)} %v_hbm.1, bf16[1,128]{1,0:T(2,128)(2,1)} %bitcast.11, bf16[128,256]{1,0:T(8,128)(2,1)} %stream_hbm.1, f32[1,256]{1,0:T(1,128)} %bitcast.8, s32[2,128]{1,0:T(2,128)} %bitcast.9, ...), custom_call_target="tpu_custom_call" | custom-call | tf_op jit(solution)/shard_map/pallas_call | solution.py:860
  71.3 1.5 %copy.17 = bf16[128,256]{1,0:T(8,128)(2,1)} copy(bf16[128,256]{1,0:T(8,128)(2,1)} %shard_map.145) | data formatting | bytes 131072
